TPU v7x, 128 devices: a whole 4x4x4 slice. The times are simulated.
128 devices in a mesh: dp: 4 (over x), kv: 16 (over z, y), tp: 2 (over core).
Axes of the slice: x: 4, y: 4, z: 4, core: 2. Of those that a mesh axis runs over, the one named last changes fastest.
Arguments:
- layer_input: bfloat16 [512, 4096], P('dp', ('kv', 'tp')), parts along dimension 0, may hold values from -22 to 22
- gate_weight: bfloat16 [4096, 2048], P(('kv', 'tp')), may hold values from -0.09375 to 0.09375
- value_weight: bfloat16 [4096, 2048], P(('kv', 'tp')), may hold values from -0.09375 to 0.09375
- write_weight: bfloat16 [4096, 256], P(('kv', 'tp')), may hold values from -0.09375 to 0.09375
- read_weight: bfloat16 [4096, 256], P(('kv', 'tp')), may hold values from -0.09375 to 0.09375
- step_weight: bfloat16 [4096, 32], P(('kv', 'tp')), may hold values from -0.09375 to 0.09375
- value_taps: bfloat16 [4, 2048], replicated, may hold values from -3 to 3
- write_taps: bfloat16 [4, 256], replicated, may hold values from -3 to 3
- read_taps: bfloat16 [4, 256], replicated, may hold values from -3 to 3
- past_values: bfloat16 [512, 3, 2048], P(('dp', 'kv', 'tp')), parts along dimension 0, may hold values from -6 to 6
- past_writes: bfloat16 [512, 3, 256], P(('dp', 'kv', 'tp')), parts along dimension 0, may hold values from -6 to 6
- past_reads: bfloat16 [512, 3, 256], P(('dp', 'kv', 'tp')), parts along dimension 0, may hold values from -6 to 6
- step_bias: float32 [32], replicated, may hold values from -4 to -1
- decay_log: float32 [32], replicated, may hold values from 0 to 2.77
- skip_scale: float32 [32], replicated, may hold values from 0.5 to 2
- state_past: float32 [512, 32, 64, 128], P(('dp', 'kv', 'tp')), parts along dimension 0, may hold values from -3 to 3
- mixer_gain: float32 [2048], replicated, may hold values from 0.1 to 1.9
- out_weight: bfloat16 [2048, 4096], P(None, ('kv', 'tp')), may hold values from -0.125 to 0.125
- norm1_gain: float32 [4096], replicated, may hold values from 0.24 to 3.7
- up_weight: bfloat16 [4096, 16384], P(None, ('kv', 'tp')), may hold values from -0.09375 to 0.09375
- down_weight: bfloat16 [16384, 4096], P(('kv', 'tp')), may hold values from -0.09375 to 0.09375
- norm2_gain: float32 [4096], replicated, may hold values from 0.1 to 1.9
Outputs:
- layer_output: bfloat16 [512, 4096], P('dp', ('kv', 'tp')), parts along dimension 0
- state_next: float32 [512, 32, 64, 128], P(('dp', 'kv', 'tp')), parts along dimension 0
There are 4 independent parts, one for each index of `dp`. A program takes and returns all parts, laid end to end along the dimension named above; an argument that names none is the same for every part. Nothing has to cross between parts.
All inputs are finite; a program needn't handle non-finite values.
Results may differ from a plain program's by a relative error of at most 0.012.
Values may be sent and summed in bfloat16 or wider, within the bound.
No kernel may reach another device: no remote copies, remote signals or barrier semaphores. Data moves between devices by JAX's collectives and lax.ppermute only.
A program may use at most 64 MiB of HBM per device.

v0:
```python
import jax
import jax.numpy as jnp
from jax import lax
from jax.sharding import PartitionSpec as P

HEADS = 32
HEAD_DIM = 64
STATE_DIM = 128
GROUPS = 2


RESIDUAL_SCALE = 2.0**0.25
NORM_EPSILON = 1e-05
MIXER_EPSILON = 1e-06


def cut_along(value, dim, devices):
    shape = value.shape
    parts = value.reshape(*shape[:dim], devices, shape[dim] // devices, *shape[dim + 1 :])
    return jnp.moveaxis(parts, dim, 0)


def sent_and_summed(value, axis, dim):
    parts = cut_along(value, dim, lax.axis_size(axis))
    arrived = lax.all_to_all(parts, axis, split_axis=0, concat_axis=0, tiled=True)
    return arrived.astype(jnp.float32).sum(axis=0)


def copy_for_each(value, axis):
    copies = jnp.broadcast_to(value, (lax.axis_size(axis), *value.shape))
    return lax.all_to_all(copies, axis, split_axis=0, concat_axis=0, tiled=True)


def joined_along(parts, dim):
    parts = jnp.moveaxis(parts, 0, dim)
    shape = parts.shape
    return parts.reshape(*shape[:dim], shape[dim] * shape[dim + 1], *shape[dim + 2 :])


def gather_directly(value, axis, dim):
    parts = copy_for_each(value, axis)
    return joined_along(parts, dim)


def sent_and_summed_2(value, axis, dim):
    parts = cut_along(value, dim, lax.axis_size(axis))
    arrived = lax.all_to_all(parts, axis, split_axis=0, concat_axis=0, tiled=True)
    return arrived.sum(axis=0)


def of_everyone(value, axis):
    return copy_for_each(value, axis).sum(axis=0)


def packed_total(arrays, axis):
    ends = [0]
    for a in arrays:
        ends.append(ends[-1] + a.size)
    total = of_everyone(jnp.concatenate([a.ravel() for a in arrays]), axis)
    return tuple((total[b:e].reshape(a.shape) for a, b, e in zip(arrays, ends, ends[1:])))


def conv_silu(current, earlier, kernel):
    stacked = jnp.concatenate([earlier, current[:, None, :]], 1).astype(jnp.float32)
    return jax.nn.silu(jnp.sum(stacked * kernel.astype(jnp.float32)[None], 1))


def mixer_step(
    gate,
    values,
    writes,
    reads,
    steps,
    value_taps,
    write_taps,
    read_taps,
    past_values,
    past_writes,
    past_reads,
    step_bias,
    decay_log,
    skip_scale,
    state_past,
    mixer_gain,
):
    seq_count = gate.shape[0]
    values_act = conv_silu(values, past_values, value_taps).reshape(seq_count, HEADS, HEAD_DIM)
    writes_act = conv_silu(writes, past_writes, write_taps).reshape(seq_count, GROUPS, STATE_DIM)
    reads_act = conv_silu(reads, past_reads, read_taps).reshape(seq_count, GROUPS, STATE_DIM)
    per_group = HEADS // GROUPS
    writes_head = jnp.repeat(writes_act, per_group, axis=1)
    reads_head = jnp.repeat(reads_act, per_group, axis=1)
    step_size = jax.nn.softplus(steps.astype(jnp.float32) + step_bias)
    decays = jnp.exp(-step_size * jnp.exp(decay_log))
    state_next = (
        decays[:, :, None, None] * state_past
        + (step_size[:, :, None] * values_act)[:, :, :, None] * writes_head[:, :, None, :]
    )
    readout = jnp.einsum("shpn,shn->shp", state_next, reads_head, precision=lax.Precision.HIGHEST)
    readout = readout + skip_scale[None, :, None] * values_act
    gated = readout.reshape(seq_count, HEADS * HEAD_DIM) * jax.nn.silu(gate.astype(jnp.float32))
    grouped = gated.reshape(seq_count, GROUPS, -1)
    grouped = grouped * lax.rsqrt(jnp.mean(jnp.square(grouped), -1, keepdims=True) + MIXER_EPSILON)
    mixed = (grouped.reshape(seq_count, -1) * mixer_gain).astype(jnp.bfloat16)
    return (mixed, state_next)


def layer_norm(rows, gain):
    average = jnp.mean(rows, -1, keepdims=True)
    variance = jnp.mean(jnp.square(rows - average), -1, keepdims=True)
    return (rows - average) * lax.rsqrt(variance + NORM_EPSILON) * gain


def norm_from_sums(rows, row_sums, full_width, gain):
    average = row_sums[0][:, None] / full_width
    variance = row_sums[1][:, None] / full_width - average * average
    return (rows - average) * lax.rsqrt(variance + NORM_EPSILON) * gain


def on_device(
    layer_input,
    gate_weight,
    value_weight,
    write_weight,
    read_weight,
    step_weight,
    value_taps,
    write_taps,
    read_taps,
    past_values,
    past_writes,
    past_reads,
    step_bias,
    decay_log,
    skip_scale,
    state_past,
    mixer_gain,
    out_weight,
    norm1_gain,
    up_weight,
    down_weight,
    norm2_gain,
):
    width_here = layer_input.shape[1]
    full_width = norm1_gain.shape[0]
    device_slot = lax.axis_index(("kv", "tp"))
    weights = (gate_weight, value_weight, write_weight, read_weight, step_weight)

    def input_terms():
        pieces = [
            jnp.dot(layer_input, weight, preferred_element_type=jnp.float32) for weight in weights
        ]
        return jnp.concatenate(pieces, 1)

    projected = sent_and_summed(input_terms().astype(jnp.bfloat16), ("kv", "tp"), 0).astype(
        jnp.bfloat16
    )
    bounds = [0]
    for weight in weights:
        bounds.append(bounds[-1] + weight.shape[1])
    gate, values, writes, reads, steps = [
        projected[:, bounds[index] : bounds[index + 1]] for index in range(5)
    ]
    mixed, state_next = mixer_step(
        gate,
        values,
        writes,
        reads,
        steps,
        value_taps,
        write_taps,
        read_taps,
        past_values,
        past_writes,
        past_reads,
        step_bias,
        decay_log,
        skip_scale,
        state_past,
        mixer_gain,
    )
    mix_out = jnp.dot(
        gather_directly(mixed, ("kv", "tp"), 0), out_weight, preferred_element_type=jnp.float32
    ).astype(jnp.bfloat16)
    residual = RESIDUAL_SCALE * layer_input.astype(jnp.float32) + mix_out.astype(jnp.float32)
    whole_residual = gather_directly(residual, ("kv", "tp"), 1)
    normed_all = layer_norm(whole_residual, norm1_gain).astype(jnp.bfloat16)
    normed_own = lax.dynamic_slice_in_dim(normed_all, device_slot * width_here, width_here, 1)
    hidden = jnp.square(
        jax.nn.relu(jnp.dot(normed_all, up_weight, preferred_element_type=jnp.float32))
    ).astype(jnp.bfloat16)
    channel_terms = jnp.dot(hidden, down_weight, preferred_element_type=jnp.float32)
    channel = sent_and_summed_2(channel_terms, ("kv", "tp"), 1).astype(jnp.bfloat16)
    second = RESIDUAL_SCALE * normed_own.astype(jnp.float32) + channel.astype(jnp.float32)
    out_sums = packed_total((jnp.sum(second, 1), jnp.sum(second * second, 1)), ("kv", "tp"))
    gain_last = lax.dynamic_slice_in_dim(norm2_gain, device_slot * width_here, width_here, 0)
    result = norm_from_sums(second, out_sums, full_width, gain_last).astype(jnp.bfloat16)
    return (result, state_next)


def solution(mesh):
    placed = (
        P("dp", ("kv", "tp")),
        P(("kv", "tp"), None),
        P(("kv", "tp"), None),
        P(("kv", "tp"), None),
        P(("kv", "tp"), None),
        P(("kv", "tp"), None),
        P(),
        P(),
        P(),
        P(("dp", "kv", "tp"), None, None),
        P(("dp", "kv", "tp"), None, None),
        P(("dp", "kv", "tp"), None, None),
        P(),
        P(),
        P(),
        P(("dp", "kv", "tp"), None, None, None),
        P(),
        P(None, ("kv", "tp")),
        P(),
        P(None, ("kv", "tp")),
        P(("kv", "tp"), None),
        P(),
    )
    return jax.shard_map(
        on_device,
        mesh=mesh,
        in_specs=placed,
        out_specs=(P("dp", ("kv", "tp")), P(("dp", "kv", "tp"), None, None, None)),
        check_vma=False,
    )
```

profile of v0, /device:TPU:1, one launch (start us, length us, event | category | flops | bytes accessed | tf_op | source)
XLA Modules:
  0.0 153.7 jit_solution(11887470797458168645)
XLA Ops:
  0.7 1.0 copy-done
  1.7 1.0 convolution_convert_fusion.1
  3.0 1.0 constant_dynamic-update-slice_fusion.4
  5.2 1.0 constant_dynamic-update-slice_fusion.3
  6.2 0.7 constant_dynamic-update-slice_fusion.2
  6.9 0.7 constant_dynamic-update-slice_fusion.1
  7.5 0.6 constant_dynamic-update-slice_fusion
  8.2 9.6 %all-to-all-start = ((bf16[32,4,4640]{2,1,0:T(4,128)(2,1)}), bf16[32,4,4640]{2,1,0:T(4,128)(2,1)S(1)}, u32[]{:S(2)}, u32[]{:S(2)}) async-start(bf16[32,4,4640]{2,1,0:T(4,128)(2,1)} %constant_dynamic-update-slice_fusion), calls=%async_computation | async-start | bytes 2424832 | tf_op jit(solution)/shard_map/all_to_all | solution.py:25
  17.9 18.3 %all-to-all-done = bf16[32,4,4640]{2,1,0:T(4,128)(2,1)S(1)} async-done(((bf16[32,4,4640]{2,1,0:T(4,128)(2,1)}), bf16[32,4,4640]{2,1,0:T(4,128)(2,1)S(1)}, u32[]{:S(2)}, u32[]{:S(2)}) %all-to-all-start) | async-done | bytes 1187872 | tf_op jit(solution)/shard_map/all_to_all | solution.py:25
  37.2 3.7 %multiply_add_fusion = f32[4,32,64,128]{3,2,1,0:T(8,128)S(1)} fusion(f32[4,32,64,128]{3,2,1,0:T(8,128)} %param.37, f32[4,32,128]{2,1,0:T(8,128)S(1)} %bitcast.62, f32[4,32,64]{2,1,0:T(8,128)S(1)} %broadcast_multiply_fusion, f32[4,32]{1,0:T(4,128)S(1)} %get-tuple-element.4), kind=kLoop, calls=%fused_computation | loop fusion | flops 3145728 | bytes 8487424 | tf_op jit(solution)/shard_map/add | solution.py:96
  40.9 6.6 %fusion.16 = f32[4,32,1,64]{3,2,1,0:T(1,128)S(1)} fusion(f32[4,32,64,128]{3,2,1,0:T(8,128)S(1)} %multiply_add_fusion, f32[4,32,128,1]{2,3,1,0:T(1,128)S(1)} %bitcast.63), kind=kOutput, calls=%fused_computation.59 | convolution fusion | flops 12582912 | bytes 4292608 | tf_op jit(solution)/shard_map/shpn,shn->shp/dot_general | solution.py:99
  48.3 15.4 %all_to_all.26 = bf16[32,4,2048]{2,1,0:T(4,128)(2,1)S(1)} all-to-all(bf16[32,4,2048]{2,1,0:T(4,128)(2,1)S(1)} %broadcast_in_dim.21), channel_id=1, replica_groups=mesh['dp'=4,'kv'=16,'tp'=2] {'kv','tp'}, dimensions={0} | all-to-all | bytes 1048576 | tf_op jit(solution)/shard_map/all_to_all | solution.py:31
  64.4 31.9 %all_to_all.27 = f32[32,128,128]{2,1,0:T(8,128)S(1)} all-to-all(f32[32,128,128]{2,1,0:T(8,128)S(1)} %broadcast_in_dim.22), channel_id=1, replica_groups=mesh['dp'=4,'kv'=16,'tp'=2] {'kv','tp'}, dimensions={0} | all-to-all | bytes 4194304 | tf_op jit(solution)/shard_map/all_to_all | solution.py:31
  97.0 1.3 fusion.2
  98.4 5.2 %convolution_bitcast_fusion = f32[16,32,8,128]{3,2,1,0:T(8,128)S(1)} fusion(bf16[512,4096]{1,0:T(8,128)(2,1)} %param.42, bf16[128,4096]{1,0:T(8,128)(2,1)} %fusion.2, bf16[4096,512]{1,0:T(8,128)(2,1)} %param.41), kind=kOutput, calls=%fused_computation.11 | convolution fusion | flops 1073938432 | bytes 11534336 | tf_op jit(solution)/shard_map/dot_general | solution.py:192
  103.5 1.6 %copy.46 = f32[16,32,8,128]{3,2,0,1:T(8,128)} copy(f32[16,32,8,128]{3,2,1,0:T(8,128)S(1)} %convolution_bitcast_fusion) | data formatting | bytes 4194304 | tf_op jit(solution)/shard_map/reshape | solution.py:19
  105.1 4.1 %all-to-all-start.3 = ((f32[32,128,128]{2,1,0:T(8,128)}), f32[32,128,128]{2,1,0:T(8,128)S(1)}, u32[]{:S(2)}, u32[]{:S(2)}) async-start(f32[32,128,128]{2,1,0:T(8,128)} %bitcast.60), calls=%async_computation.3 | async-start | bytes 4194304 | tf_op jit(solution)/shard_map/all_to_all | solution.py:47
  109.2 28.3 %all-to-all-done.3 = f32[32,128,128]{2,1,0:T(8,128)S(1)} async-done(((f32[32,128,128]{2,1,0:T(8,128)}), f32[32,128,128]{2,1,0:T(8,128)S(1)}, u32[]{:S(2)}, u32[]{:S(2)}) %all-to-all-start.3) | async-done | bytes 2097184 | tf_op jit(solution)/shard_map/all_to_all | solution.py:47
  137.6 0.9 fusion.10
  138.5 0.6 broadcast_in_dim.23
  139.1 5.6 %all-to-all-start.4 = ((f32[32,1,256]{2,1,0:T(1,128)}), f32[32,1,256]{2,1,0:T(1,128)S(1)}, u32[]{:S(2)}, u32[]{:S(2)}) async-start(f32[32,1,256]{2,1,0:T(1,128)} %broadcast_in_dim.23), calls=%async_computation.4 | async-start | bytes 65536 | tf_op jit(solution)/shard_map/all_to_all | solution.py:31
  144.8 0.8 dynamic_slice.7
  145.6 6.6 %all-to-all-done.4 = f32[32,1,256]{2,1,0:T(1,128)S(1)} async-done(((f32[32,1,256]{2,1,0:T(1,128)}), f32[32,1,256]{2,1,0:T(1,128)S(1)}, u32[]{:S(2)}, u32[]{:S(2)}) %all-to-all-start.4) | async-done | bytes 32800 | tf_op jit(solution)/shard_map/all_to_all | solution.py:31
  152.2 1.5 multiply_convert_fusion
  (85 shorter events, 4.5 us)
Async XLA Ops:
  0.6 1.0 copy-start
  0.6 3.3 %copy-start.2 = (bf16[128,128]{1,0:T(8,128)(2,1)S(1)}, bf16[128,128]{1,0:T(8,128)(2,1)}, u32[]{:S(2)}) copy-start(bf16[128,128]{1,0:T(8,128)(2,1)} %param.22) | copy-start | bytes 98308
  0.7 3.3 %copy-start.3 = (bf16[128,2048]{1,0:T(8,128)(2,1)S(1)}, bf16[128,2048]{1,0:T(8,128)(2,1)}, u32[]{:S(2)}) copy-start(bf16[128,2048]{1,0:T(8,128)(2,1)} %param.24) | copy-start | bytes 1572868
  2.7 1.8 %copy-start.5 = (bf16[128,256]{1,0:T(8,128)(2,1)S(1)}, bf16[128,256]{1,0:T(8,128)(2,1)}, u32[]{:S(2)}) copy-start(bf16[128,256]{1,0:T(8,128)(2,1)} %param.25) | copy-start | bytes 196612
  2.7 1.9 %copy-start.6 = (bf16[128,256]{1,0:T(8,128)(2,1)S(1)}, bf16[128,256]{1,0:T(8,128)(2,1)}, u32[]{:S(2)}) copy-start(bf16[128,256]{1,0:T(8,128)(2,1)} %param.26) | copy-start | bytes 196612
  3.0 2.0 %copy-start.10 = (bf16[128,32]{0,1:T(8,128)(2,1)S(1)}, bf16[128,32]{0,1:T(8,128)(2,1)}, u32[]{:S(2)}) copy-start(bf16[128,32]{0,1:T(8,128)(2,1)} %param.27) | copy-start | bytes 24580
  4.7 13.1 %copy-start.14 = (bf16[4,256]{1,0:T(4,128)(2,1)S(1)}, bf16[4,256]{1,0:T(4,128)(2,1)}, u32[]{:S(2)}) copy-start(bf16[4,256]{1,0:T(4,128)(2,1)} %param.29) | copy-start | bytes 6148
  4.7 13.1 %copy-start.15 = (bf16[4,256]{1,0:T(4,128)(2,1)S(1)}, bf16[4,256]{1,0:T(4,128)(2,1)}, u32[]{:S(2)}) copy-start(bf16[4,256]{1,0:T(4,128)(2,1)} %param.30) | copy-start | bytes 6148
  4.7 13.1 %copy-start.9 = (bf16[4,2048]{1,0:T(4,128)(2,1)S(1)}, bf16[4,2048]{1,0:T(4,128)(2,1)}, u32[]{:S(2)}) copy-start(bf16[4,2048]{1,0:T(4,128)(2,1)} %param.28) | copy-start | bytes 49156
  4.7 13.1 %copy-start.18 = (f32[32]{0:T(128)S(1)}, f32[32]{0:T(128)}, u32[]{:S(2)}) copy-start(f32[32]{0:T(128)} %param.35) | copy-start | bytes 388
  6.2 30.5 %copy-start.12 = (bf16[4,3,256]{2,0,1:T(4,128)(2,1)S(1)}, bf16[4,3,256]{2,0,1:T(4,128)(2,1)}, u32[]{:S(2)}) copy-start(bf16[4,3,256]{2,0,1:T(4,128)(2,1)} %param.33) | copy-start | bytes 18436
  6.2 30.5 %copy-start.13 = (bf16[4,3,256]{2,0,1:T(4,128)(2,1)S(1)}, bf16[4,3,256]{2,0,1:T(4,128)(2,1)}, u32[]{:S(2)}) copy-start(bf16[4,3,256]{2,0,1:T(4,128)(2,1)} %param.32) | copy-start | bytes 18436
  6.2 30.6 %copy-start.7 = (bf16[4,3,2048]{2,0,1:T(4,128)(2,1)S(1)}, bf16[4,3,2048]{2,0,1:T(4,128)(2,1)}, u32[]{:S(2)}) copy-start(bf16[4,3,2048]{2,0,1:T(4,128)(2,1)} %param.31) | copy-start | bytes 147460
  7.5 29.5 %copy-start.17 = (f32[32]{0:T(128)S(1)}, f32[32]{0:T(128)}, u32[]{:S(2)}) copy-start(f32[32]{0:T(128)} %param.34) | copy-start | bytes 388
  8.2 28.0 %all-to-all-start = ((bf16[32,4,4640]{2,1,0:T(4,128)(2,1)}), bf16[32,4,4640]{2,1,0:T(4,128)(2,1)S(1)}, u32[]{:S(2)}, u32[]{:S(2)}) async-start(bf16[32,4,4640]{2,1,0:T(4,128)(2,1)} %constant_dynamic-update-slice_fusion), calls=%async_computation | async-start | bytes 2424832 | tf_op jit(solution)/shard_map/all_to_all | solution.py:25
  40.9 6.6 %copy-start.1 = (f32[4,32,64,128]{3,2,1,0:T(8,128)}, f32[4,32,64,128]{3,2,1,0:T(8,128)S(1)}, u32[]{:S(2)}) copy-start(f32[4,32,64,128]{3,2,1,0:T(8,128)S(1)} %multiply_add_fusion) | copy-start | bytes 12582916
  40.9 6.6 %copy-start.16 = (f32[32]{0:T(128)S(1)}, f32[32]{0:T(128)}, u32[]{:S(2)}) copy-start(f32[32]{0:T(128)} %param.36) | copy-start | bytes 388
  40.9 7.1 %copy-start.11 = (f32[2048]{0:T(1024)S(1)}, f32[2048]{0:T(1024)}, u32[]{:S(2)}) copy-start(f32[2048]{0:T(1024)} %param.38) | copy-start | bytes 24580
  47.5 16.3 %copy-start.4 = (bf16[2048,128]{1,0:T(8,128)(2,1)S(1)}, bf16[2048,128]{1,0:T(8,128)(2,1)}, u32[]{:S(2)}) copy-start(bf16[2048,128]{1,0:T(8,128)(2,1)} %param.39) | copy-start | bytes 1572868
  96.3 0.7 copy-start.8
  105.1 32.4 %all-to-all-start.3 = ((f32[32,128,128]{2,1,0:T(8,128)}), f32[32,128,128]{2,1,0:T(8,128)S(1)}, u32[]{:S(2)}, u32[]{:S(2)}) async-start(f32[32,128,128]{2,1,0:T(8,128)} %bitcast.60), calls=%async_computation.3 | async-start | bytes 4194304 | tf_op jit(solution)/shard_map/all_to_all | solution.py:47
  139.1 13.0 %all-to-all-start.4 = ((f32[32,1,256]{2,1,0:T(1,128)}), f32[32,1,256]{2,1,0:T(1,128)S(1)}, u32[]{:S(2)}, u32[]{:S(2)}) async-start(f32[32,1,256]{2,1,0:T(1,128)} %broadcast_in_dim.23), calls=%async_computation.4 | async-start | bytes 65536 | tf_op jit(solution)/shard_map/all_to_all | solution.py:31
where the time goes:
time: 154 us
  waiting for transfers between devices  53.2 us (35%)
  blocking collectives  47.3 us (31%)
  starting transfers between devices  19.3 us (13%)
  matrix products  13.8 us (9%)
  local copies, waits for them, and re-layouts  9.8 us (6%)
  other arithmetic  9.18 us (6%)
    all_to_all x2, blocking collectives, copy_for_each(): return lax.all_to_all(copies, axis, split_axis=0, concat_axis=0, tiled=True)  47.3 us
    all_to_all x1, waiting for transfers between devices, sent_and_summed_2(): lax.all_to_all(parts, axis, split_axis=0, concat_axis=0, tiled=True)  28.3 us
    all_to_all x1, waiting for transfers between devices, sent_and_summed(): lax.all_to_all(parts, axis, split_axis=0, concat_axis=0, tiled=True)  18.3 us
    all_to_all x1, starting transfers between devices, sent_and_summed(): lax.all_to_all(parts, axis, split_axis=0, concat_axis=0, tiled=True)  9.59 us
    all_to_all x1, waiting for transfers between devices, copy_for_each(): return lax.all_to_all(copies, axis, split_axis=0, concat_axis=0, tiled=True)  6.6 us
    dot_general x1, matrix products, mixer_step(): jnp.einsum('shpn,shn->shp', state_next, reads_head, precision=lax.Precisi...  6.59 us
    all_to_all x1, starting transfers between devices, copy_for_each(): return lax.all_to_all(copies, axis, split_axis=0, concat_axis=0, tiled=True)  5.64 us
    dot_general x1, matrix products, on_device(): jnp.dot(hidden, down_weight, preferred_element_type=jnp.float32)  5.16 us
  transfers between devices with their start and end apart: 3, of which 3 were waited for; matrix products, arithmetic and copies ran while one was open for 1% of the time, Pallas kernels for 0%

commit v1 on v0

v1 whole, which is shorter than its diff:
```python
import jax
import jax.numpy as jnp
from jax import lax
from jax.sharding import PartitionSpec as P

HEADS = 32
HEAD_DIM = 64
STATE_DIM = 128
GROUPS = 2
RESIDUAL_SCALE = 2.0**0.25
NORM_EPSILON = 1e-05
MIXER_EPSILON = 1e-06
SWAP = [(0, 1), (1, 0)]


def other_core(value):
    return lax.ppermute(value, "tp", SWAP)


def exchange(parts, axis):
    return lax.all_to_all(parts, axis, split_axis=0, concat_axis=0, tiled=True)


def copies_from(value, axis):
    return exchange(jnp.broadcast_to(value, (lax.axis_size(axis), *value.shape)), axis)


def conv_silu(current, earlier, kernel):
    stacked = jnp.concatenate([earlier, current[:, None, :]], 1).astype(jnp.float32)
    return jax.nn.silu(jnp.sum(stacked * kernel.astype(jnp.float32)[None], 1))


def mixer_step(
    gate,
    values,
    writes,
    reads,
    steps,
    value_taps,
    write_taps,
    read_taps,
    past_values,
    past_writes,
    past_reads,
    step_bias,
    decay_log,
    skip_scale,
    state_past,
    mixer_gain,
):
    seq_count = gate.shape[0]
    values_act = conv_silu(values, past_values, value_taps).reshape(seq_count, HEADS, HEAD_DIM)
    writes_act = conv_silu(writes, past_writes, write_taps).reshape(seq_count, GROUPS, STATE_DIM)
    reads_act = conv_silu(reads, past_reads, read_taps).reshape(seq_count, GROUPS, STATE_DIM)
    per_group = HEADS // GROUPS
    writes_head = jnp.repeat(writes_act, per_group, axis=1)
    reads_head = jnp.repeat(reads_act, per_group, axis=1)
    step_size = jax.nn.softplus(steps.astype(jnp.float32) + step_bias)
    decays = jnp.exp(-step_size * jnp.exp(decay_log))
    state_next = (
        decays[:, :, None, None] * state_past
        + (step_size[:, :, None] * values_act)[:, :, :, None] * writes_head[:, :, None, :]
    )
    readout = jnp.sum(state_next * reads_head[:, :, None, :], -1)
    readout = readout + skip_scale[None, :, None] * values_act
    gated = readout.reshape(seq_count, HEADS * HEAD_DIM) * jax.nn.silu(gate.astype(jnp.float32))
    grouped = gated.reshape(seq_count, GROUPS, -1)
    grouped = grouped * lax.rsqrt(jnp.mean(jnp.square(grouped), -1, keepdims=True) + MIXER_EPSILON)
    mixed = (grouped.reshape(seq_count, -1) * mixer_gain).astype(jnp.bfloat16)
    return (mixed, state_next)


def layer_norm(rows, gain):
    average = jnp.mean(rows, -1, keepdims=True)
    variance = jnp.mean(jnp.square(rows - average), -1, keepdims=True)
    return (rows - average) * lax.rsqrt(variance + NORM_EPSILON) * gain


def on_device(
    layer_input,
    gate_weight,
    value_weight,
    write_weight,
    read_weight,
    step_weight,
    value_taps,
    write_taps,
    read_taps,
    past_values,
    past_writes,
    past_reads,
    step_bias,
    decay_log,
    skip_scale,
    state_past,
    mixer_gain,
    out_weight,
    norm1_gain,
    up_weight,
    down_weight,
    norm2_gain,
):
    core = lax.axis_index("tp")
    chip = lax.axis_index("kv")
    chips = lax.axis_size("kv")
    width = norm1_gain.shape[0]
    rows = layer_input.shape[0] // (2 * chips)
    half = chips * rows
    weights = (gate_weight, value_weight, write_weight, read_weight, step_weight)

    input_rows = layer_input.reshape(chips, 2, rows, -1)
    own_input = lax.dynamic_index_in_dim(input_rows, core, 1, False).reshape(half, -1)
    far_input = lax.dynamic_index_in_dim(input_rows, 1 - core, 1, False).reshape(half, -1)

    def input_terms(of_rows):
        pieces = [jnp.dot(of_rows, weight, preferred_element_type=jnp.float32) for weight in weights]
        return jnp.concatenate(pieces, 1)

    arrived = other_core(input_terms(far_input).astype(jnp.bfloat16))
    terms = (input_terms(own_input) + arrived.astype(jnp.float32)).astype(jnp.bfloat16)
    projected = exchange(terms.reshape(chips, rows, -1), "kv").astype(jnp.float32).sum(0)
    projected = projected.astype(jnp.bfloat16)
    bounds = [0]
    for weight in weights:
        bounds.append(bounds[-1] + weight.shape[1])
    gate, values, writes, reads, steps = [
        projected[:, bounds[index] : bounds[index + 1]] for index in range(5)
    ]
    mixed, state_next = mixer_step(
        gate,
        values,
        writes,
        reads,
        steps,
        value_taps,
        write_taps,
        read_taps,
        past_values,
        past_writes,
        past_reads,
        step_bias,
        decay_log,
        skip_scale,
        state_past,
        mixer_gain,
    )
    own_mixed = copies_from(mixed, "kv").reshape(half, -1)
    far_mixed = other_core(own_mixed)

    def residual_of(mixed_rows, input_of_rows):
        mix_out = jnp.dot(mixed_rows, out_weight, preferred_element_type=jnp.float32)
        return (RESIDUAL_SCALE * input_of_rows.astype(jnp.float32) + mix_out).astype(jnp.bfloat16)

    def in_order(own, far, dim):
        first = jnp.where(core == 0, own, far)
        second = jnp.where(core == 0, far, own)
        return jnp.stack([first, second], dim)

    residual = in_order(residual_of(own_mixed, own_input), residual_of(far_mixed, far_input), 0)
    residual = residual.reshape(2 * half, -1)
    own_columns = copies_from(residual, "kv")
    far_columns = other_core(own_columns)
    whole = in_order(own_columns, far_columns, 1)
    whole = jnp.moveaxis(whole, 2, 0).reshape(2 * half, width).astype(jnp.float32)
    normed = layer_norm(whole, norm1_gain).astype(jnp.bfloat16)
    hidden = jnp.square(
        jax.nn.relu(jnp.dot(normed, up_weight, preferred_element_type=jnp.float32))
    ).astype(jnp.bfloat16)
    channel_terms = jnp.dot(hidden, down_weight, preferred_element_type=jnp.float32)
    own_terms = lax.dynamic_slice_in_dim(channel_terms, core * half, half, 0)
    far_terms = lax.dynamic_slice_in_dim(channel_terms, (1 - core) * half, half, 0)
    arrived = other_core(far_terms.astype(jnp.bfloat16))
    terms = (own_terms + arrived.astype(jnp.float32)).astype(jnp.bfloat16)
    channel = exchange(terms.reshape(chips, rows, width), "kv").astype(jnp.float32).sum(0)
    normed_own = lax.dynamic_slice_in_dim(normed, core * half + chip * rows, rows, 0)
    second = RESIDUAL_SCALE * normed_own.astype(jnp.float32) + channel
    result = layer_norm(second, norm2_gain).astype(jnp.bfloat16)
    result = jnp.moveaxis(result.reshape(rows, 2 * chips, -1), 1, 0)
    result = exchange(result, ("kv", "tp")).reshape(2 * half, -1)
    return (result, state_next)


def solution(mesh):
    placed = (
        P("dp", ("kv", "tp")),
        P(("kv", "tp"), None),
        P(("kv", "tp"), None),
        P(("kv", "tp"), None),
        P(("kv", "tp"), None),
        P(("kv", "tp"), None),
        P(),
        P(),
        P(),
        P(("dp", "kv", "tp"), None, None),
        P(("dp", "kv", "tp"), None, None),
        P(("dp", "kv", "tp"), None, None),
        P(),
        P(),
        P(),
        P(("dp", "kv", "tp"), None, None, None),
        P(),
        P(None, ("kv", "tp")),
        P(),
        P(None, ("kv", "tp")),
        P(("kv", "tp"), None),
        P(),
    )
    return jax.shard_map(
        on_device,
        mesh=mesh,
        in_specs=placed,
        out_specs=(P("dp", ("kv", "tp")), P(("dp", "kv", "tp"), None, None, None)),
        check_vma=False,
    )
```

time: 154 us -> 115 us (0.75)
  waiting for transfers between devices: 53.2 us -> 27.2 us
  blocking collectives: 47.3 us -> 35.8 us
  other arithmetic: 9.18 us -> 15.7 us
  local copies, waits for them, and re-layouts: 9.8 us -> 6.43 us
  matrix products: 13.8 us -> 10.7 us
  starting transfers between devices: 19.3 us -> 17.6 us
    all_to_all x3 -> x2, waiting for transfers between devices: 53.2 us -> 22.3 us  [exchange(): return lax.all_to_all(parts, axis, split_axis=0, concat_axis=0, tiled=True)]
    all_to_all x2 -> x3, blocking collectives: 47.3 us -> 35.8 us  [exchange(): return lax.all_to_all(parts, axis, split_axis=0, concat_axis=0, tiled=True)]
    all_to_all x3 -> x2, starting transfers between devices: 19.3 us -> 11.5 us  [exchange(): return lax.all_to_all(parts, axis, split_axis=0, concat_axis=0, tiled=True)]
    ppermute x0 -> x4, starting transfers between devices: none -> 6.19 us  [other_core(): return lax.ppermute(value, 'tp', SWAP)]
    reduce_sum x4 -> x3, other arithmetic: 1.55 us -> 6.8 us  [the longest x1 6.33 us: mixer_step(): readout = jnp.sum(state_next * reads_head[:, :, None, :], -1)]
    ppermute x0 -> x4, waiting for transfers between devices: none -> 4.9 us  [other_core(): return lax.ppermute(value, 'tp', SWAP)]
    unnamed x44 -> x39, local copies, waits for them, and re-layouts: 4.71 us -> 0.82 us
    add x2 -> x0, other arithmetic: 3.81 us -> none  [the longest x1 3.73 us: mixer_step(): decays[:, :, None, None] * state_past]
  transfers between devices with their start and end apart: 3 -> 6, of which waited for: 3 -> 6; matrix products, arithmetic and copies ran while one was open for 1% -> 1% of each run, Pallas kernels for 0% -> 0%
where the time goes in v1:
time: 115 us
  blocking collectives  35.8 us (31%)
  waiting for transfers between devices  27.2 us (24%)
  starting transfers between devices  17.6 us (15%)
  other arithmetic  15.7 us (14%)
  matrix products  10.7 us (9%)
  local copies, waits for them, and re-layouts  6.43 us (6%)
    all_to_all x3, blocking collectives, exchange(): return lax.all_to_all(parts, axis, split_axis=0, concat_axis=0, tiled=True)  35.8 us
    all_to_all x2, waiting for transfers between devices, exchange(): return lax.all_to_all(parts, axis, split_axis=0, concat_axis=0, tiled=True)  22.3 us
    all_to_all x2, starting transfers between devices, exchange(): return lax.all_to_all(parts, axis, split_axis=0, concat_axis=0, tiled=True)  11.5 us
    reduce_sum x1, other arithmetic, mixer_step(): readout = jnp.sum(state_next * reads_head[:, :, None, :], -1)  6.33 us
    ppermute x4, starting transfers between devices, other_core(): return lax.ppermute(value, 'tp', SWAP)  6.19 us
    dot_general x1, matrix products, on_device(): jnp.dot(hidden, down_weight, preferred_element_type=jnp.float32)  5.16 us
    dot_general x10, matrix products, input_terms(): jnp.dot(of_rows, weight, preferred_element_type=jnp.float32)  5.09 us
    ppermute x4, waiting for transfers between devices, other_core(): return lax.ppermute(value, 'tp', SWAP)  4.9 us
  transfers between devices with their start and end apart: 6, of which 6 were waited for; matrix products, arithmetic and copies ran while one was open for 1% of the time, Pallas kernels for 0%

profile of v1, /device:TPU:1, one launch (start us, length us, event | category | flops | bytes accessed | tf_op | source)
XLA Modules:
  0.0 114.6 jit_solution(16217897443613597122)
XLA Ops:
  2.7 1.3 %fusion = bf16[64,4640]{1,0:T(8,128)(2,1)S(1)} fusion(bf16[64,4640]{1,0:T(8,128)(2,1)S(1)} %fusion.1, bf16[64,128]{1,0:T(8,128)(2,1)S(1)} %bitcast.73, bf16[128,2048]{1,0:T(8,128)(2,1)} %param.24), kind=kOutput, calls=%fused_computation.5 | convolution fusion | flops 33685504 | bytes 802816 | tf_op jit(solution)/shard_map/dot_general | solution.py:116
  4.0 1.0 fusion.5
  5.0 1.0 fusion.4
  6.0 1.5 %collective-permute-start = (bf16[64,4640]{1,0:T(8,128)(2,1)S(1)}, bf16[64,4640]{1,0:T(8,128)(2,1)S(1)}, u32[]{:S(2)}, u32[]{:S(2)}) collective-permute-start(bf16[64,4640]{1,0:T(8,128)(2,1)S(1)} %constant_dynamic-update-slice_fusion), channel_id=1, source_target_pairs={{0,1},{1,0},{2,3},{3,2},{4,5},{5,4},{6,7},{7,6},{8,9},{9,8},{10,11... | collective-permute-start | bytes 1781768 | tf_op jit(solution)/shard_map/ppermute | solution.py:17
  9.2 1.0 reshape.115
  10.2 7.9 %all-to-all-start = ((bf16[16,4,4640]{2,1,0:T(4,128)(2,1)}), bf16[16,4,4640]{2,1,0:T(4,128)(2,1)S(1)}, u32[]{:S(2)}, u32[]{:S(2)}) async-start(bf16[16,4,4640]{2,1,0:T(4,128)(2,1)} %reshape.115), calls=%async_computation | async-start | bytes 1212416 | tf_op jit(solution)/shard_map/all_to_all | solution.py:21
  18.3 11.4 %all-to-all-done = bf16[16,4,4640]{2,1,0:T(4,128)(2,1)S(1)} async-done(((bf16[16,4,4640]{2,1,0:T(4,128)(2,1)}), bf16[16,4,4640]{2,1,0:T(4,128)(2,1)S(1)}, u32[]{:S(2)}, u32[]{:S(2)}) %all-to-all-start) | async-done | bytes 593952 | tf_op jit(solution)/shard_map/all_to_all | solution.py:21
  30.4 6.3 %multiply_reduce_fusion = (f32[4,32,64]{2,1,0:T(8,128)S(1)}, f32[4,32,64,128]{3,2,1,0:T(8,128)}) fusion(f32[4,32,128]{2,1,0:T(8,128)S(1)} %bitcast.78, f32[4,32,128]{2,1,0:T(8,128)S(1)} %bitcast.77, f32[4,32,64]{2,1,0:T(8,128)S(1)} %multiply_multiply_fusion, f32[4,32,64,128]{3,2,1,0:T(8,128)} %param.37, f32[4,32]{1,0:T(4,128)S(1)} %get-tuple-element.8), kind=kLoop, calls=%fused_computation | loop fusion | flops 5234688 | bytes 8585728 | tf_op jit(solution)/shard_map/reduce_sum | solution.py:64
  37.3 10.8 %all_to_all.25 = bf16[16,4,2048]{2,1,0:T(4,128)(2,1)S(1)} all-to-all(bf16[16,4,2048]{2,1,0:T(4,128)(2,1)S(1)} %broadcast_in_dim.19), channel_id=1, replica_groups=mesh['dp'=4,'kv'=16,'tp'=2] {'kv'}, dimensions={0} | all-to-all | bytes 524288 | tf_op jit(solution)/shard_map/all_to_all | solution.py:21
  48.2 2.5 %collective-permute-start.1 = (bf16[64,2048]{1,0:T(8,128)(2,1)S(1)}, bf16[64,2048]{1,0:T(8,128)(2,1)S(1)}, u32[]{:S(2)}, u32[]{:S(2)}) collective-permute-start(bf16[64,2048]{1,0:T(8,128)(2,1)S(1)} %reshape.116), channel_id=1, source_target_pairs={{0,1},{1,0},{2,3},{3,2},{4,5},{5,4},{6,7},{7,6},{8,9},{9,8},{10,11... | collective-permute-start | bytes 786440 | tf_op jit(solution)/shard_map/ppermute | solution.py:17
  52.3 13.3 %all_to_all.26 = bf16[16,128,128]{1,2,0:T(8,128)(2,1)S(1)} all-to-all(bf16[16,128,128]{1,2,0:T(8,128)(2,1)S(1)} %broadcast_in_dim.20), channel_id=1, replica_groups=mesh['dp'=4,'kv'=16,'tp'=2] {'kv'}, dimensions={0} | all-to-all | bytes 1048576 | tf_op jit(solution)/shard_map/all_to_all | solution.py:21
  65.7 1.8 %collective-permute-start.2 = (bf16[16,128,128]{1,2,0:T(8,128)(2,1)S(1)}, bf16[16,128,128]{1,2,0:T(8,128)(2,1)S(1)}, u32[]{:S(2)}, u32[]{:S(2)}) collective-permute-start(bf16[16,128,128]{1,2,0:T(8,128)(2,1)S(1)} %all_to_all.26), channel_id=1, source_target_pairs={{0,1},{1,0},{2,3},{3,2},{4,5},{5,4},{6,7},{7,6},{8,9},{9,8},{10,11... | collective-permute-start | bytes 1572872 | tf_op jit(solution)/shard_map/ppermute | solution.py:17
  67.5 1.5 %collective-permute-done.2 = bf16[16,128,128]{1,2,0:T(8,128)(2,1)S(1)} collective-permute-done((bf16[16,128,128]{1,2,0:T(8,128)(2,1)S(1)}, bf16[16,128,128]{1,2,0:T(8,128)(2,1)S(1)}, u32[]{:S(2)}, u32[]{:S(2)}) %collective-permute-start.2) | collective-permute-done | bytes 524320 | tf_op jit(solution)/shard_map/ppermute | solution.py:17
  70.4 1.9 %copy.49 = f32[128,4096]{1,0:T(8,128)} copy(f32[128,4096]{0,1:T(8,128)S(1)} %bitcast.64) | data formatting | bytes 4194304 | tf_op jit(solution)/shard_map/convert_element_type | solution.py:164
  72.2 2.9 %multiply_convert_fusion = bf16[128,4096]{1,0:T(8,128)(2,1)} fusion(f32[128,4096]{1,0:T(8,128)} %copy.49, f32[4096]{0:T(1024)S(1)} %copy-done.7, f32[128]{0:T(128)S(1)} %add_rsqrt_fusion.2, f32[128]{0:T(128)S(1)} %broadcast_multiply_fusion.1), kind=kLoop, calls=%fused_computation.8 | loop fusion | flops 2097152 | bytes 3163136 | tf_op jit(solution)/shard_map/convert_element_type | solution.py:165
  75.1 5.2 %fusion.8 = f32[128,4096]{1,0:T(8,128)S(1)} fusion(bf16[512,4096]{1,0:T(8,128)(2,1)} %param.42, bf16[128,4096]{1,0:T(8,128)(2,1)} %multiply_convert_fusion, bf16[4096,512]{1,0:T(8,128)(2,1)} %param.41), kind=kOutput, calls=%fused_computation.26 | convolution fusion | flops 1073938432 | bytes 11534336 | tf_op jit(solution)/shard_map/dot_general | solution.py:169
  80.8 1.7 %collective-permute-done.3 = bf16[64,4096]{1,0:T(8,128)(2,1)} collective-permute-done((bf16[64,4096]{1,0:T(8,128)(2,1)S(1)}, bf16[64,4096]{1,0:T(8,128)(2,1)}, u32[]{:S(2)}, u32[]{:S(2)}) %collective-permute-start.3) | collective-permute-done | bytes 524320 | tf_op jit(solution)/shard_map/ppermute | solution.py:17
  82.5 1.1 add_convert_fusion.1
  83.6 1.0 reshape.118
  84.6 3.6 %all-to-all-start.3 = ((bf16[16,4,4096]{2,1,0:T(4,128)(2,1)}), bf16[16,4,4096]{2,1,0:T(4,128)(2,1)S(1)}, u32[]{:S(2)}, u32[]{:S(2)}) async-start(bf16[16,4,4096]{2,1,0:T(4,128)(2,1)} %reshape.118), calls=%async_computation.3 | async-start | bytes 1048576 | tf_op jit(solution)/shard_map/all_to_all | solution.py:21
  88.2 10.9 %all-to-all-done.3 = bf16[16,4,4096]{2,1,0:T(4,128)(2,1)S(1)} async-done(((bf16[16,4,4096]{2,1,0:T(4,128)(2,1)}), bf16[16,4,4096]{2,1,0:T(4,128)(2,1)S(1)}, u32[]{:S(2)}, u32[]{:S(2)}) %all-to-all-start.3) | async-done | bytes 524320 | tf_op jit(solution)/shard_map/all_to_all | solution.py:21
  99.3 1.0 fusion.16
  100.3 1.1 multiply_reduce_fusion.3
  102.3 11.6 %all_to_all.27 = bf16[32,4,128]{2,1,0:T(4,128)(2,1)S(1)} all-to-all(bf16[32,4,128]{2,1,0:T(4,128)(2,1)S(1)} %fusion.14), channel_id=1, replica_groups=mesh['dp'=4,'kv'=16,'tp'=2] {'kv','tp'}, dimensions={0} | all-to-all | bytes 65536 | tf_op jit(solution)/shard_map/all_to_all | solution.py:21
  (97 shorter events, 10.4 us)
Async XLA Ops:
  0.6 1.9 %copy-start = (bf16[128,2048]{1,0:T(8,128)(2,1)S(1)}, bf16[128,2048]{1,0:T(8,128)(2,1)}, u32[]{:S(2)}) copy-start(bf16[128,2048]{1,0:T(8,128)(2,1)} %param.23) | copy-start | bytes 1572868
  0.6 7.0 %copy-start.1 = (bf16[128,2048]{1,0:T(8,128)(2,1)S(1)}, bf16[128,2048]{1,0:T(8,128)(2,1)}, u32[]{:S(2)}) copy-start(bf16[128,2048]{1,0:T(8,128)(2,1)} %param.24) | copy-start | bytes 1572868
  0.7 7.2 %copy-start.3 = (bf16[128,256]{1,0:T(8,128)(2,1)S(1)}, bf16[128,256]{1,0:T(8,128)(2,1)}, u32[]{:S(2)}) copy-start(bf16[128,256]{1,0:T(8,128)(2,1)} %param.25) | copy-start | bytes 196612
  1.5 6.5 %copy-start.4 = (bf16[128,256]{1,0:T(8,128)(2,1)S(1)}, bf16[128,256]{1,0:T(8,128)(2,1)}, u32[]{:S(2)}) copy-start(bf16[128,256]{1,0:T(8,128)(2,1)} %param.26) | copy-start | bytes 196612
  2.5 5.7 %copy-start.6 = (bf16[128,32]{0,1:T(8,128)(2,1)S(1)}, bf16[128,32]{0,1:T(8,128)(2,1)}, u32[]{:S(2)}) copy-start(bf16[128,32]{0,1:T(8,128)(2,1)} %param.27) | copy-start | bytes 24580
  6.0 3.1 %collective-permute-start = (bf16[64,4640]{1,0:T(8,128)(2,1)S(1)}, bf16[64,4640]{1,0:T(8,128)(2,1)S(1)}, u32[]{:S(2)}, u32[]{:S(2)}) collective-permute-start(bf16[64,4640]{1,0:T(8,128)(2,1)S(1)} %constant_dynamic-update-slice_fusion), channel_id=1, source_target_pairs={{0,1},{1,0},{2,3},{3,2},{4,5},{5,4},{6,7},{7,6},{8,9},{9,8},{10,11... | collective-permute-start | bytes 1781768 | tf_op jit(solution)/shard_map/ppermute | solution.py:17
  8.3 9.8 %copy-start.17 = (f32[32]{0:T(128)S(1)}, f32[32]{0:T(128)}, u32[]{:S(2)}) copy-start(f32[32]{0:T(128)} %param.35) | copy-start | bytes 388
  8.3 9.8 %copy-start.13 = (bf16[4,256]{1,0:T(4,128)(2,1)S(1)}, bf16[4,256]{1,0:T(4,128)(2,1)}, u32[]{:S(2)}) copy-start(bf16[4,256]{1,0:T(4,128)(2,1)} %param.29) | copy-start | bytes 6148
  8.3 9.8 %copy-start.14 = (bf16[4,256]{1,0:T(4,128)(2,1)S(1)}, bf16[4,256]{1,0:T(4,128)(2,1)}, u32[]{:S(2)}) copy-start(bf16[4,256]{1,0:T(4,128)(2,1)} %param.30) | copy-start | bytes 6148
  8.3 9.9 %copy-start.15 = (f32[32]{0:T(128)S(1)}, f32[32]{0:T(128)}, u32[]{:S(2)}) copy-start(f32[32]{0:T(128)} %param.36) | copy-start | bytes 388
  8.3 10.0 %copy-start.8 = (bf16[4,2048]{1,0:T(4,128)(2,1)S(1)}, bf16[4,2048]{1,0:T(4,128)(2,1)}, u32[]{:S(2)}) copy-start(bf16[4,2048]{1,0:T(4,128)(2,1)} %param.28) | copy-start | bytes 49156
  9.2 20.8 %copy-start.11 = (bf16[4,3,256]{2,0,1:T(4,128)(2,1)S(1)}, bf16[4,3,256]{2,0,1:T(4,128)(2,1)}, u32[]{:S(2)}) copy-start(bf16[4,3,256]{2,0,1:T(4,128)(2,1)} %param.33) | copy-start | bytes 18436
  9.2 20.8 %copy-start.12 = (bf16[4,3,256]{2,0,1:T(4,128)(2,1)S(1)}, bf16[4,3,256]{2,0,1:T(4,128)(2,1)}, u32[]{:S(2)}) copy-start(bf16[4,3,256]{2,0,1:T(4,128)(2,1)} %param.32) | copy-start | bytes 18436
  9.2 20.9 %copy-start.5 = (bf16[4,3,2048]{2,0,1:T(4,128)(2,1)S(1)}, bf16[4,3,2048]{2,0,1:T(4,128)(2,1)}, u32[]{:S(2)}) copy-start(bf16[4,3,2048]{2,0,1:T(4,128)(2,1)} %param.31) | copy-start | bytes 147460
  9.2 21.0 %copy-start.16 = (f32[32]{0:T(128)S(1)}, f32[32]{0:T(128)}, u32[]{:S(2)}) copy-start(f32[32]{0:T(128)} %param.34) | copy-start | bytes 388
  10.2 19.5 %all-to-all-start = ((bf16[16,4,4640]{2,1,0:T(4,128)(2,1)}), bf16[16,4,4640]{2,1,0:T(4,128)(2,1)S(1)}, u32[]{:S(2)}, u32[]{:S(2)}) async-start(bf16[16,4,4640]{2,1,0:T(4,128)(2,1)} %reshape.115), calls=%async_computation | async-start | bytes 1212416 | tf_op jit(solution)/shard_map/all_to_all | solution.py:21
  30.4 6.8 %copy-start.10 = (f32[2048]{0:T(1024)S(1)}, f32[2048]{0:T(1024)}, u32[]{:S(2)}) copy-start(f32[2048]{0:T(1024)} %param.38) | copy-start | bytes 24580
  30.4 20.3 %copy-start.2 = (bf16[2048,128]{1,0:T(8,128)(2,1)S(1)}, bf16[2048,128]{1,0:T(8,128)(2,1)}, u32[]{:S(2)}) copy-start(bf16[2048,128]{1,0:T(8,128)(2,1)} %param.39) | copy-start | bytes 1572868
  48.2 3.7 %collective-permute-start.1 = (bf16[64,2048]{1,0:T(8,128)(2,1)S(1)}, bf16[64,2048]{1,0:T(8,128)(2,1)S(1)}, u32[]{:S(2)}, u32[]{:S(2)}) collective-permute-start(bf16[64,2048]{1,0:T(8,128)(2,1)S(1)} %reshape.116), channel_id=1, source_target_pairs={{0,1},{1,0},{2,3},{3,2},{4,5},{5,4},{6,7},{7,6},{8,9},{9,8},{10,11... | collective-permute-start | bytes 786440 | tf_op jit(solution)/shard_map/ppermute | solution.py:17
  65.7 3.3 %collective-permute-start.2 = (bf16[16,128,128]{1,2,0:T(8,128)(2,1)S(1)}, bf16[16,128,128]{1,2,0:T(8,128)(2,1)S(1)}, u32[]{:S(2)}, u32[]{:S(2)}) collective-permute-start(bf16[16,128,128]{1,2,0:T(8,128)(2,1)S(1)} %all_to_all.26), channel_id=1, source_target_pairs={{0,1},{1,0},{2,3},{3,2},{4,5},{5,4},{6,7},{7,6},{8,9},{9,8},{10,11... | collective-permute-start | bytes 1572872 | tf_op jit(solution)/shard_map/ppermute | solution.py:17
  70.3 1.9 %copy-start.7 = (f32[4096]{0:T(1024)S(1)}, f32[4096]{0:T(1024)}, u32[]{:S(2)}) copy-start(f32[4096]{0:T(1024)} %param.40) | copy-start | bytes 49156
  80.4 2.1 %collective-permute-start.3 = (bf16[64,4096]{1,0:T(8,128)(2,1)S(1)}, bf16[64,4096]{1,0:T(8,128)(2,1)}, u32[]{:S(2)}, u32[]{:S(2)}) collective-permute-start(bf16[64,4096]{1,0:T(8,128)(2,1)S(1)} %dynamic-slice_convert_fusion), channel_id=1, source_target_pairs={{0,1},{1,0},{2,3},{3,2},{4,5},{5,4},{6,7},{7,6},{8,9},{9,8},{10,11... | collective-permute-start | bytes 1572872 | tf_op jit(solution)/shard_map/ppermute | solution.py:17
  80.8 20.6 %copy-start.9 = (f32[4096]{0:T(1024)S(1)}, f32[4096]{0:T(1024)}, u32[]{:S(2)}) copy-start(f32[4096]{0:T(1024)} %param.43) | copy-start | bytes 49156
  84.6 14.5 %all-to-all-start.3 = ((bf16[16,4,4096]{2,1,0:T(4,128)(2,1)}), bf16[16,4,4096]{2,1,0:T(4,128)(2,1)S(1)}, u32[]{:S(2)}, u32[]{:S(2)}) async-start(bf16[16,4,4096]{2,1,0:T(4,128)(2,1)} %reshape.118), calls=%async_computation.3 | async-start | bytes 1048576 | tf_op jit(solution)/shard_map/all_to_all | solution.py:21

commit v2 on v1

v2 whole, which is shorter than its diff:
```python
import jax
import jax.numpy as jnp
from jax import lax
from jax.experimental import pallas as pl
from jax.experimental.pallas import tpu as pltpu
from jax.sharding import PartitionSpec as P

HEADS = 32
HEAD_DIM = 64
STATE_DIM = 128
GROUPS = 2
RESIDUAL_SCALE = 2.0**0.25
NORM_EPSILON = 1e-05
MIXER_EPSILON = 1e-06
SWAP = [(0, 1), (1, 0)]
LANES = 128
F32 = jnp.float32
BF16 = jnp.bfloat16
NT = (((1,), (1,)), ((), ()))


def other_core(value):
    return lax.ppermute(value, "tp", SWAP)


def exchange(parts, axis):
    return lax.all_to_all(parts, axis, split_axis=0, concat_axis=0, tiled=True)


def kernel(body, outs, args, out_space=pltpu.VMEM, in_spaces=None, scratch=(), flops=0, limit=24):
    in_spaces = in_spaces or [pltpu.VMEM] * len(args)
    return pl.pallas_call(
        body,
        name=body.__name__,
        in_specs=[pl.BlockSpec(memory_space=space) for space in in_spaces],
        out_specs=[pl.BlockSpec(memory_space=out_space)] * len(outs),
        out_shape=[out_space(shape, dtype) for shape, dtype in outs],
        scratch_shapes=list(scratch),
        compiler_params=pltpu.CompilerParams(vmem_limit_bytes=limit * 2**20),
        cost_estimate=pl.CostEstimate(flops=flops, bytes_accessed=0, transcendentals=0),
    )(*[pltpu.with_memory_space_constraint(a, s) for a, s in zip(args, in_spaces)])


def dot(a, b):
    return jnp.dot(a, b, preferred_element_type=F32)


def sigmoid(value):
    return 1.0 / (1.0 + jnp.exp(-value))


def upper_rows(shape):
    return lax.broadcasted_iota(jnp.int32, shape, 0) % 8 < 4


def total_of(ref):
    total = ref[0].astype(F32)
    for j in range(1, ref.shape[0]):
        total = total + ref[j].astype(F32)
    return total


def project_rows(
    x_hbm,
    gate_hbm,
    value_hbm,
    write_hbm,
    read_hbm,
    step_hbm,
    far_ref,
    own_ref,
    order_ref,
    x_ref,
    gate_ref,
    value_ref,
    write_ref,
    read_ref,
    step_ref,
    rows_ref,
    arrivals,
):
    core = lax.axis_index("tp")
    pairs = (
        (x_hbm, x_ref),
        (step_hbm, step_ref.at[pl.ds(0, step_hbm.shape[0])]),
        (write_hbm, write_ref),
        (read_hbm, read_ref),
        (gate_hbm, gate_ref),
        (value_hbm, value_ref),
    )
    copies = [
        pltpu.make_async_copy(src, dst, arrivals.at[n]) for n, (src, dst) in enumerate(pairs)
    ]
    for copy in copies:
        copy.start()
    copies[0].wait()
    rows_ref[0] = x_ref[...].astype(F32)
    half = order_ref.shape[0] // 2
    for k in range(x_ref.shape[0] // 8):
        for c in range(2):
            order_ref[c * half + 4 * k : c * half + 4 * k + 4, :] = (
                RESIDUAL_SCALE * rows_ref[0, 8 * k + 4 * c : 8 * k + 4 * c + 4, :]
            )
        own = rows_ref[0, pl.ds(8 * k + 4 * core, 4), :]
        far = rows_ref[0, pl.ds(8 * k + 4 * (1 - core), 4), :]
        for place, value in ((1, own), (2, far)):
            rows_ref[place, pl.ds(8 * k, 4), :] = value
            rows_ref[place, pl.ds(8 * k + 4, 4), :] = value
    own = rows_ref[1].astype(BF16)
    far = rows_ref[2].astype(BF16)
    copies[1].wait()
    step_ref[step_hbm.shape[0] :, :] = jnp.zeros(
        (step_ref.shape[0] - step_hbm.shape[0], step_ref.shape[1]), BF16
    )
    inner, group = gate_ref.shape[1], write_ref.shape[1]
    for rows, out_ref in ((far, far_ref), (own, own_ref)):
        steps = lax.dot_general(rows, step_ref[...], NT, preferred_element_type=F32)
        steps = jnp.where(upper_rows(steps.shape), steps, 0.0)
        out_ref[:, :, inner + group :] = steps.astype(out_ref.dtype).reshape(-1, 8, LANES)
    copies[2].wait()
    copies[3].wait()
    for rows, out_ref in ((far, far_ref), (own, own_ref)):
        first, second = dot(rows, write_ref[...]), dot(rows, read_ref[...])
        both = jnp.where(upper_rows(first.shape), first, second).astype(out_ref.dtype)
        out_ref[:, :, inner : inner + group] = both.reshape(-1, 8, group)
    copies[4].wait()
    copies[5].wait()
    chunk = 512
    for rows, out_ref in ((far, far_ref), (own, own_ref)):
        for n in range(inner // chunk):
            at = slice(n * chunk, (n + 1) * chunk)
            first, second = dot(rows, gate_ref[:, at]), dot(rows, value_ref[:, at])
            both = jnp.where(upper_rows(first.shape), first, second).astype(out_ref.dtype)
            out_ref[:, :, at] = both.reshape(-1, 8, chunk)


def add_terms(own_ref, arrived_ref, *rest):
    out_ref = rest[-1]
    for k in range(out_ref.shape[0]):
        out_ref[k] = (own_ref[k] + arrived_ref[k].astype(F32)).astype(BF16)


def spread_heads(rows, inner):
    shape = (rows.shape[1], inner)
    spread = lax.broadcasted_iota(jnp.int32, shape, 1) // HEAD_DIM == lax.broadcasted_iota(
        jnp.int32, shape, 0
    )
    return dot(rows, spread.astype(F32).astype(BF16))


def prepare(
    state_hbm,
    past_value_hbm,
    past_write_hbm,
    past_read_hbm,
    value_taps_hbm,
    write_taps_hbm,
    read_taps_hbm,
    bias_hbm,
    rate_hbm,
    skip_hbm,
    state_ref,
    past_ref,
    taps_ref,
    head_ref,
    states_ref,
    past_value_ref,
    past_write_ref,
    past_read_ref,
    value_taps_ref,
    write_taps_ref,
    read_taps_ref,
    bias_ref,
    rate_ref,
    skip_ref,
    arrivals,
    state_arrivals,
):
    pairs = (
        (past_value_hbm, past_value_ref),
        (past_write_hbm, past_write_ref),
        (past_read_hbm, past_read_ref),
        (value_taps_hbm, value_taps_ref),
        (write_taps_hbm, write_taps_ref),
        (read_taps_hbm, read_taps_ref),
        (bias_hbm, bias_ref),
        (rate_hbm, rate_ref),
        (skip_hbm, skip_ref),
    )
    copies = [
        pltpu.make_async_copy(src, dst, arrivals.at[n]) for n, (src, dst) in enumerate(pairs)
    ]
    for copy in copies:
        copy.start()
    pieces = state_arrivals.shape[0]
    rows = state_ref.shape[0] // pieces
    state_copies = []
    for n in range(pieces):
        at = pl.ds(n * rows, rows)
        state_copies.append(
            pltpu.make_async_copy(state_hbm.at[at], states_ref.at[at], state_arrivals.at[n])
        )
        state_copies[-1].start()
    for copy in copies:
        copy.wait()
    at = 0
    for old_ref, tap_ref in (
        (past_value_ref, value_taps_ref),
        (past_write_ref, write_taps_ref),
        (past_read_ref, read_taps_ref),
    ):
        width = tap_ref.shape[1]
        taps = tap_ref[...].astype(F32)
        total = old_ref[0].astype(F32) * taps[0:1]
        for k in range(1, old_ref.shape[0]):
            total = total + old_ref[k].astype(F32) * taps[k : k + 1]
        past_ref[:, at : at + width] = total
        taps_ref[:, at : at + width] = taps[old_ref.shape[0] :]
        at += width
    heads = jnp.concatenate([bias_ref[...], jnp.exp(rate_ref[...]), skip_ref[...]], 0)
    terms = jnp.concatenate(split_terms(heads, 3), 0).astype(BF16)
    wide = spread_heads(terms, head_ref.shape[1])
    head_ref[...] = wide[0:3] + wide[3:6] + wide[6:9]
    for n in range(pieces):
        state_copies[n].wait()
        at = slice(n * rows, (n + 1) * rows)
        state_ref[at, :] = states_ref[at, :].astype(BF16)


def fetch(after_ref, up_hbm, up_ref, arrivals):
    pieces = arrivals.shape[0]
    rows = up_hbm.shape[0] // pieces
    copies = []
    for n in range(pieces):
        at = pl.ds(n * rows, rows)
        copies.append(pltpu.make_async_copy(up_hbm.at[at], up_ref.at[at], arrivals.at[n]))
        copies[-1].start()
    for copy in copies:
        copy.wait()


def mix(
    arrived_ref, past_ref, taps_ref, head_ref, gain_ref, state_ref, out_ref, decay_ref, drive_ref, write_ref
):
    inner = gain_ref.shape[1]
    seqs = out_ref.shape[1]
    group = inner // GROUPS
    span = GROUPS * STATE_DIM
    total = total_of(arrived_ref).astype(BF16).astype(F32)
    gate = total[:seqs, :inner]
    steps = total[:seqs, inner + span : inner + span + HEADS].astype(BF16)

    def active(new, at):
        conv = past_ref[:, at] + taps_ref[:, at] * new
        return conv * sigmoid(conv)

    values = active(total[seqs:, :inner], slice(0, inner))
    writes = active(total[:seqs, inner : inner + span], slice(inner, inner + span))
    reads = active(total[seqs:, inner : inner + span], slice(inner + span, inner + 2 * span))
    raw = spread_heads(steps, inner) + head_ref[0:1, :]
    step_size = jnp.maximum(raw, 0.0) + jnp.log1p(jnp.exp(-jnp.abs(raw)))
    decay = jnp.exp(-step_size * head_ref[1:2, :])
    drive = step_size * values
    high = reads.astype(BF16).astype(F32)
    low = reads - high
    row = lax.broadcasted_iota(jnp.int32, (seqs, group), 0)
    recalled, overlap = [], []
    for g in range(GROUPS):
        at = slice(g * STATE_DIM, (g + 1) * STATE_DIM)
        query = jnp.concatenate([high[:, at], low[:, at]], 0).astype(BF16)
        part = jnp.zeros((seqs, group), F32)
        for s in range(seqs):
            base = (s * GROUPS + g) * group
            found = lax.dot_general(query, state_ref[base : base + group, :], NT, preferred_element_type=F32)
            part = jnp.where(row == s, found[:seqs] + found[seqs:], part)
        recalled.append(part)
        both = jnp.sum(writes[:, at] * reads[:, at], 1, keepdims=True)
        overlap.append(jnp.broadcast_to(both, (seqs, group)))
    readout = (
        decay * jnp.concatenate(recalled, 1)
        + drive * jnp.concatenate(overlap, 1)
        + head_ref[2:3, :] * values
    )
    gated = readout * (gate * sigmoid(gate))
    normed = []
    for g in range(GROUPS):
        cut = gated[:, g * group : (g + 1) * group]
        mean = jnp.sum(cut * cut, 1, keepdims=True) * (1.0 / group)
        normed.append(cut * lax.rsqrt(mean + MIXER_EPSILON))
    mixed = (jnp.concatenate(normed, 1) * gain_ref[...]).astype(BF16)
    for k in range(out_ref.shape[0]):
        out_ref[k] = mixed
    decay_ref[...] = decay
    drive_ref[...] = drive
    write_ref[...] = writes


def split_terms(value, count):
    terms = []
    for _ in range(count):
        terms.append(value.astype(BF16).astype(F32))
        value = value - terms[-1]
    return terms


def next_state(
    state_hbm, decay_ref, drive_ref, write_ref, out_hbm, state_ref, out_ref, arrivals, departures
):
    seqs, inner = decay_ref.shape
    group = inner // GROUPS
    copies, loads = [], []
    for n in range(seqs * GROUPS):
        span = pl.ds(n * group, group)
        loads.append(pltpu.make_async_copy(state_hbm.at[span], state_ref.at[span], arrivals.at[n]))
        loads[-1].start()
    for s in range(seqs):
        for g in range(GROUPS):
            at = slice(g * group, (g + 1) * group)
            decay = split_terms(decay_ref[s : s + 1, at], 3)
            drive = split_terms(drive_ref[s : s + 1, at], 2)
            write = split_terms(write_ref[s : s + 1, g * STATE_DIM : (g + 1) * STATE_DIM], 2)
            one = jnp.ones((1, STATE_DIM), F32)
            blank_left, blank_right = jnp.zeros((5, group), F32), jnp.zeros((5, STATE_DIM), F32)
            left = jnp.concatenate([*decay, blank_left], 0).T.astype(BF16)
            right = jnp.concatenate([one, one, one, blank_right], 0).astype(BF16)
            factor = dot(left, right)
            left = jnp.concatenate([drive[0], drive[1], drive[0], blank_left], 0).T.astype(BF16)
            right = jnp.concatenate([write[0], write[0], write[1], blank_right], 0).astype(BF16)
            added = dot(left, right)
            base = (s * GROUPS + g) * group
            rows = slice(base, base + group)
            loads[s * GROUPS + g].wait()
            out_ref[rows, :] = factor * state_ref[rows, :] + added
            span = pl.ds(base, group)
            copies.append(
                pltpu.make_async_copy(
                    out_ref.at[span], out_hbm.at[span], departures.at[len(copies)]
                )
            )
            copies[-1].start()
    for copy in copies:
        copy.wait()


def channel_mixer(
    own_ref,
    far_ref,
    gain_ref,
    up_ref,
    down_hbm,
    far_out_ref,
    own_out_ref,
    row_ref,
    normed_ref,
    down_ref,
    arrivals,
):
    pieces = arrivals.shape[0]
    span = down_hbm.shape[0] // pieces
    copies = []
    for n in range(pieces):
        at = pl.ds(n * span, span)
        copies.append(pltpu.make_async_copy(down_hbm.at[at], down_ref.at[at], arrivals.at[n]))
        copies[-1].start()
    core = lax.axis_index("tp")
    chip = lax.axis_index("kv")
    chips, rows_all, lanes = own_ref.shape
    half = rows_all // 2
    width = 2 * chips * lanes
    total = jnp.zeros((rows_all, lanes), F32)
    for k in range(chips):
        total = total + own_ref[k].astype(F32) + far_ref[k].astype(F32)
    mean = jnp.sum(total, 1, keepdims=True) * (1.0 / width)
    square = jnp.zeros((rows_all, lanes), F32)
    for k in range(chips):
        a = own_ref[k].astype(F32) - mean
        b = far_ref[k].astype(F32) - mean
        square = square + a * a + b * b
    scale = lax.rsqrt(jnp.sum(square, 1, keepdims=True) * (1.0 / width) + NORM_EPSILON)
    for k in range(chips):
        own = own_ref[k].astype(F32)
        far = far_ref[k].astype(F32)
        pair = (jnp.where(core == 0, own, far), jnp.where(core == 0, far, own))
        for c in range(2):
            at = slice((2 * k + c) * lanes, (2 * k + c + 1) * lanes)
            normed_ref[:, at] = ((pair[c] - mean) * scale * gain_ref[:, at]).astype(BF16)
    hidden = jnp.maximum(dot(normed_ref[...], up_ref[...]), 0.0)
    hidden = (hidden * hidden).astype(BF16)
    for copy in copies:
        copy.wait()
    chunk = 256
    upper = upper_rows((half, chunk))
    for n in range(width // 2 // chunk):
        at = slice(n * chunk, (n + 1) * chunk)
        first = dot(hidden, down_ref[:, at])
        second = dot(hidden, down_ref[:, width // 2 + n * chunk : width // 2 + (n + 1) * chunk])
        for out_ref, here in ((far_out_ref, core == 1), (own_out_ref, core == 0)):
            a = jnp.where(here, first[:half], first[half:])
            b = jnp.where(here, second[:half], second[half:])
            even = jnp.where(upper, a, pltpu.roll(b, 4, 0)).astype(out_ref.dtype)
            odd = jnp.where(upper, pltpu.roll(a, half - 4, 0), b).astype(out_ref.dtype)
            for r in range(half // 8):
                out_ref[2 * r, :, at] = even[8 * r : 8 * r + 8]
                out_ref[2 * r + 1, :, at] = odd[8 * r : 8 * r + 8]
    shape = (8, rows_all)
    wanted = core * half + chip * 4 + lax.broadcasted_iota(jnp.int32, shape, 0) % 4
    pick = wanted == lax.broadcasted_iota(jnp.int32, shape, 1)
    rows = dot(pick.astype(F32).astype(BF16), normed_ref[...])
    row_ref[...] = jnp.where(
        upper_rows(row_ref.shape), rows[:, : width // 2], rows[:, width // 2 :]
    )


def last_norm(arrived_ref, row_ref, gain_ref, out_ref):
    second = RESIDUAL_SCALE * row_ref[...] + total_of(arrived_ref)
    half = second.shape[1]

    def row_mean(value):
        sums = jnp.broadcast_to(jnp.sum(value, 1, keepdims=True), (8, LANES))
        sums = (sums + pltpu.roll(sums, 4, 0)) * (0.5 / half)
        return sums[:, 0:1]

    centred = second - row_mean(second)
    scale = lax.rsqrt(row_mean(centred * centred) + NORM_EPSILON)
    gain = jnp.where(upper_rows(second.shape), gain_ref[:, :half], gain_ref[:, half:])
    result = centred * scale * gain
    for j in range(half // LANES):
        both = result[:, j * LANES : (j + 1) * LANES]
        out_ref[j] = both[:4].astype(BF16)
        out_ref[half // LANES + j] = both[4:].astype(BF16)


def on_device(
    layer_input,
    gate_weight,
    value_weight,
    write_weight,
    read_weight,
    step_weight,
    value_taps,
    write_taps,
    read_taps,
    past_values,
    past_writes,
    past_reads,
    step_bias,
    decay_log,
    skip_scale,
    state_past,
    mixer_gain,
    out_weight,
    norm1_gain,
    up_weight,
    down_weight,
    norm2_gain,
):
    core = lax.axis_index("tp")
    chips = lax.axis_size("kv")
    width = norm1_gain.shape[0]
    inner = mixer_gain.shape[0]
    rows = layer_input.shape[0] // (2 * chips)
    half = chips * rows
    per_head = inner // HEADS

    span = GROUPS * STATE_DIM
    terms_width = inner + span + LANES
    far_terms, own_terms, scaled_input = kernel(
        project_rows,
        [((chips, 8, terms_width), BF16), ((chips, 8, terms_width), F32), (layer_input.shape, F32)],
        [layer_input, gate_weight, value_weight, write_weight, read_weight, step_weight.T],
        in_spaces=[pltpu.HBM] * 6,
        scratch=[
            pltpu.VMEM(layer_input.shape, BF16),
            pltpu.VMEM(gate_weight.shape, BF16),
            pltpu.VMEM(value_weight.shape, BF16),
            pltpu.VMEM(write_weight.shape, BF16),
            pltpu.VMEM(read_weight.shape, BF16),
            pltpu.VMEM((LANES, LANES), BF16),
            pltpu.VMEM((3, 2 * half, LANES), F32),
            pltpu.SemaphoreType.DMA((6,)),
        ],
        flops=2**28,
    )
    arrived = other_core(far_terms)
    state_rows = state_past.reshape(-1, STATE_DIM)
    small = [jnp.swapaxes(p, 0, 1) for p in (past_values, past_writes, past_reads)]
    small += [value_taps, write_taps, read_taps]
    small += [step_bias[None], decay_log[None], skip_scale[None]]
    conv_width = inner + 2 * span
    states, past, taps, heads = kernel(
        prepare,
        [
            (state_rows.shape, BF16),
            ((rows, conv_width), F32),
            ((1, conv_width), F32),
            ((3, inner), F32),
        ],
        [state_rows, *small],
        in_spaces=[pltpu.HBM] * 10,
        scratch=[
            pltpu.VMEM(state_rows.shape, F32),
            *[pltpu.VMEM(a.shape, a.dtype) for a in small],
            pltpu.SemaphoreType.DMA((9,)),
            pltpu.SemaphoreType.DMA((8,)),
        ],
        flops=2**29,
    )
    (terms,) = kernel(
        add_terms, [((chips, 8, terms_width), BF16)], [own_terms, arrived, taps], flops=2**20
    )
    arrived = exchange(terms, "kv")
    mixed, decay, drive, writes = kernel(
        mix,
        [
            ((chips, rows, inner), BF16),
            ((rows, inner), F32),
            ((rows, inner), F32),
            ((rows, span), F32),
        ],
        [arrived, past, taps, heads, mixer_gain[None], states],
        flops=2**28,
    )
    own_mixed = exchange(mixed, "kv").reshape(half, inner)
    far_mixed = other_core(own_mixed)

    (state_next,) = kernel(
        next_state,
        [(state_rows.shape, F32)],
        [state_rows, decay, drive, writes],
        in_spaces=[pltpu.HBM] + [pltpu.VMEM] * 3,
        out_space=pltpu.HBM,
        scratch=[
            pltpu.VMEM(state_rows.shape, F32),
            pltpu.VMEM(state_rows.shape, F32),
            pltpu.SemaphoreType.DMA((8,)),
            pltpu.SemaphoreType.DMA((8,)),
        ],
        flops=2**30,
    )
    state_next = state_next.reshape(state_past.shape)

    own_mix, far_mix = dot(own_mixed, out_weight), dot(far_mixed, out_weight)
    mix_out = jnp.concatenate(
        [jnp.where(core == 0, own_mix, far_mix), jnp.where(core == 0, far_mix, own_mix)], 0
    )
    residual = (scaled_input + mix_out).astype(BF16)
    own_columns = exchange(jnp.broadcast_to(residual, (chips, *residual.shape)), "kv")
    far_columns = other_core(own_columns)
    (up_here,) = kernel(
        fetch,
        [(up_weight.shape, BF16)],
        [own_columns, up_weight],
        in_spaces=[pltpu.VMEM, pltpu.HBM],
        scratch=[pltpu.SemaphoreType.DMA((8,))],
        flops=2**30,
        limit=4,
    )
    far_terms, own_terms, normed_rows = kernel(
        channel_mixer,
        [((chips, 8, width // 2), BF16), ((chips, 8, width // 2), F32), ((8, width // 2), F32)],
        [own_columns, far_columns, norm1_gain[None], up_here, down_weight],
        in_spaces=[pltpu.VMEM] * 4 + [pltpu.HBM],
        scratch=[
            pltpu.VMEM((2 * half, width), BF16),
            pltpu.VMEM(down_weight.shape, BF16),
            pltpu.SemaphoreType.DMA((4,)),
        ],
        flops=2**30,
    )
    arrived = other_core(far_terms)
    (terms,) = kernel(
        add_terms, [((chips, 8, width // 2), BF16)], [own_terms, arrived], flops=2**20
    )
    arrived = exchange(terms, "kv")
    (result,) = kernel(
        last_norm,
        [((2 * chips, rows, LANES), BF16)],
        [arrived, normed_rows, norm2_gain[None]],
        flops=2**20,
    )
    result = exchange(result, ("kv", "tp")).reshape(2 * half, LANES)
    return (result, state_next)


def solution(mesh):
    placed = (
        P("dp", ("kv", "tp")),
        P(("kv", "tp"), None),
        P(("kv", "tp"), None),
        P(("kv", "tp"), None),
        P(("kv", "tp"), None),
        P(("kv", "tp"), None),
        P(),
        P(),
        P(),
        P(("dp", "kv", "tp"), None, None),
        P(("dp", "kv", "tp"), None, None),
        P(("dp", "kv", "tp"), None, None),
        P(),
        P(),
        P(),
        P(("dp", "kv", "tp"), None, None, None),
        P(),
        P(None, ("kv", "tp")),
        P(),
        P(None, ("kv", "tp")),
        P(("kv", "tp"), None),
        P(),
    )
    return jax.shard_map(
        on_device,
        mesh=mesh,
        in_specs=placed,
        out_specs=(P("dp", ("kv", "tp")), P(("dp", "kv", "tp"), None, None, None)),
        check_vma=False,
    )
```

time: 115 us -> 94.4 us (0.82)
  waiting for transfers between devices: 27.2 us -> 5.11 us
  blocking collectives: 35.8 us -> 57.6 us
  Pallas kernels: 0 us -> 18.5 us
  other arithmetic: 15.7 us -> 0.01 us
  matrix products: 10.7 us -> 0.44 us
  starting transfers between devices: 17.6 us -> 10.9 us
  local copies, waits for them, and re-layouts: 6.43 us -> 0.8 us
    all_to_all x3 -> x4, blocking collectives: 35.8 us -> 57.6 us  [exchange(): return lax.all_to_all(parts, axis, split_axis=0, concat_axis=0, tiled=True)]
    all_to_all x2 -> x1, waiting for transfers between devices: 22.3 us -> 2.27 us  [exchange(): return lax.all_to_all(parts, axis, split_axis=0, concat_axis=0, tiled=True)]
    pallas_call x0 -> x9, Pallas kernels: none -> 18.5 us  [kernel(): pl.pallas_call(body, name=body.__name__, in_specs=[pl.BlockSpec(memory_sp...]
    dot_general x13 -> x2, matrix products: 10.7 us -> 0.44 us  [dot(): return jnp.dot(a, b, preferred_element_type=F32)]
    reduce_sum x10 -> x0, other arithmetic: 10.1 us -> none  [the longest x1 6.33 us: mixer_step(): readout = jnp.sum(state_next * reads_head[:, :, None, :], -1)]
    all_to_all x2 -> x1, starting transfers between devices: 11.5 us -> 5.07 us  [exchange(): return lax.all_to_all(parts, axis, split_axis=0, concat_axis=0, tiled=True)]
    convert_element_type x8 -> x1, other arithmetic: 4.33 us -> 0.01 us  [on_device(): residual = (scaled_input + mix_out).astype(BF16)]
    ppermute x4, waiting for transfers between devices: 4.9 us -> 2.83 us  [other_core(): return lax.ppermute(value, 'tp', SWAP)]
  transfers between devices with their start and end apart: 6 -> 5, of which waited for: 6 -> 3; matrix products, arithmetic and copies ran while one was open for 1% -> 0% of each run, Pallas kernels for 0% -> 10%
where the time goes in v2:
time: 94.4 us; the launch traced here: 94.1 us
  blocking collectives  57.6 us (61%)
  Pallas kernels  18.5 us (20%)
  starting transfers between devices  10.9 us (12%)
  waiting for transfers between devices  5.11 us (5%)
    all_to_all x4, blocking collectives, exchange(): return lax.all_to_all(parts, axis, split_axis=0, concat_axis=0, tiled=True)  57.6 us
    pallas_call x9, Pallas kernels, kernel(): pl.pallas_call(body, name=body.__name__, in_specs=[pl.BlockSpec(memory_sp...  18.5 us
    ppermute x4, starting transfers between devices, other_core(): return lax.ppermute(value, 'tp', SWAP)  5.8 us
    all_to_all x1, starting transfers between devices, exchange(): return lax.all_to_all(parts, axis, split_axis=0, concat_axis=0, tiled=True)  5.07 us
    ppermute x4, waiting for transfers between devices, other_core(): return lax.ppermute(value, 'tp', SWAP)  2.83 us
    all_to_all x1, waiting for transfers between devices, exchange(): return lax.all_to_all(parts, axis, split_axis=0, concat_axis=0, tiled=True)  2.27 us
  transfers between devices with their start and end apart: 5, of which 3 were waited for; matrix products, arithmetic and copies ran while one was open for 0% of the time, Pallas kernels for 10%

profile of v2, /device:TPU:1, one launch (start us, length us, event | category | flops | bytes accessed | tf_op | source)
XLA Modules:
  0.0 94.1 jit_solution(14937172371014955329)
XLA Ops:
  0.6 2.1 %project_rows.1 = (bf16[16,8,2432]{2,1,0:T(8,128)(2,1)S(1)}, f32[16,8,2432]{2,1,0:T(8,128)S(1)}, f32[128,128]{1,0:T(8,128)S(1)}) custom-call(bf16[128,128]{1,0:T(8,128)(2,1)} %x_hbm.1, bf16[128,2048]{1,0:T(8,128)(2,1)} %gate_hbm.1, bf16[128,2048]{1,0:T(8,128)(2,1)} %value_hbm.1, bf16[128,256]{1,0:T(8,128)(2,1)} %write_hbm.1, bf16[128,256]{1,0:T(8,128)(2,1)} %read_hbm.1, ...), custom_call_target="tpu_custom_call" | custom-call | flops 268435456 | tf_op jit(solution)/shard_map/project_rows/pallas_call | solution.py:32
  2.8 1.5 %collective-permute-start = (bf16[16,8,2432]{2,1,0:T(8,128)(2,1)S(1)}, bf16[16,8,2432]{2,1,0:T(8,128)(2,1)S(1)}, u32[]{:S(2)}, u32[]{:S(2)}) collective-permute-start(bf16[16,8,2432]{2,1,0:T(8,128)(2,1)S(1)} %get-tuple-element.18), channel_id=1, source_target_pairs={{0,1},{1,0},{2,3},{3,2},{4,5},{5,4},{6,7},{7,6},{8,9},{9,8},{10,11... | collective-permute-start | bytes 1867784 | tf_op jit(solution)/shard_map/ppermute | solution.py:23
  4.2 2.4 %prepare.1 = (bf16[8192,128]{1,0:T(8,128)(2,1)S(1)}, f32[4,2560]{1,0:T(4,128)S(1)}, f32[1,2560]{1,0:T(1,128)S(1)}, f32[3,2048]{1,0:T(4,128)S(1)}) custom-call(f32[8192,128]{1,0:T(8,128)} %bitcast.20, bf16[3,4,2048]{2,1,0:T(4,128)(2,1)} %bitcast.24, bf16[3,4,256]{2,1,0:T(4,128)(2,1)} %bitcast.26, bf16[3,4,256]{2,1,0:T(4,128)(2,1)} %bitcast.27, ...), custom_call_target="tpu_custom_call" | custom-call | flops 536870912 | tf_op jit(solution)/shard_map/prepare/pallas_call | solution.py:32
  6.7 0.1 add_terms.2
  6.8 20.1 %all_to_all.25.arrived_ref = bf16[16,8,2432]{2,1,0:T(8,128)(2,1)S(1)} all-to-all(bf16[16,8,2432]{2,1,0:T(8,128)(2,1)S(1)} %add_terms.2), channel_id=1, replica_groups=mesh['dp'=4,'kv'=16,'tp'=2] {'kv'}, dimensions={0} | all-to-all | bytes 1245184 | tf_op jit(solution)/shard_map/all_to_all | solution.py:27
  26.9 0.8 mix.1
  27.7 10.6 %all_to_all.26 = bf16[16,4,2048]{2,1,0:T(4,128)(2,1)S(1)} all-to-all(bf16[16,4,2048]{2,1,0:T(4,128)(2,1)S(1)} %get-tuple-element.23), channel_id=1, replica_groups=mesh['dp'=4,'kv'=16,'tp'=2] {'kv'}, dimensions={0} | all-to-all | bytes 524288 | tf_op jit(solution)/shard_map/all_to_all | solution.py:27
  38.3 2.5 %collective-permute-start.1 = (bf16[64,2048]{1,0:T(8,128)(2,1)S(1)}, bf16[64,2048]{1,0:T(8,128)(2,1)S(1)}, u32[]{:S(2)}, u32[]{:S(2)}) collective-permute-start(bf16[64,2048]{1,0:T(8,128)(2,1)S(1)} %reshape.17), channel_id=1, source_target_pairs={{0,1},{1,0},{2,3},{3,2},{4,5},{5,4},{6,7},{7,6},{8,9},{9,8},{10,11... | collective-permute-start | bytes 786440 | tf_op jit(solution)/shard_map/ppermute | solution.py:23
  40.8 0.2 fusion.1
  41.0 0.9 collective-permute-done.1
  42.0 0.2 broadcast_select_fusion.1
  42.2 0.1 broadcast_in_dim.25
  42.3 13.3 %all_to_all.27.after_ref.own_ref = bf16[16,128,128]{2,1,0:T(8,128)(2,1)S(1)} all-to-all(bf16[16,128,128]{2,1,0:T(8,128)(2,1)S(1)} %broadcast_in_dim.25), channel_id=1, replica_groups=mesh['dp'=4,'kv'=16,'tp'=2] {'kv'}, dimensions={0} | all-to-all | bytes 1048576 | tf_op jit(solution)/shard_map/all_to_all | solution.py:27
  55.7 1.8 %collective-permute-start.2 = (bf16[16,128,128]{2,1,0:T(8,128)(2,1)S(1)}, bf16[16,128,128]{2,1,0:T(8,128)(2,1)S(1)}, u32[]{:S(2)}, u32[]{:S(2)}) collective-permute-start(bf16[16,128,128]{2,1,0:T(8,128)(2,1)S(1)} %all_to_all.27.after_ref.own_ref), channel_id=1, source_target_pairs={{0,1},{1,0},{2,3},{3,2},{4,5},{5,4},{6,7},{7,6},{8,9},{9,8},{10,11... | collective-permute-start | bytes 1572872 | tf_op jit(solution)/shard_map/ppermute | solution.py:23
  57.4 2.2 %fetch.1.up_ref = bf16[4096,512]{1,0:T(8,128)(2,1)S(1)} custom-call(bf16[16,128,128]{2,1,0:T(8,128)(2,1)S(1)} %all_to_all.27.after_ref.own_ref, bf16[4096,512]{1,0:T(8,128)(2,1)} %up_hbm.1), custom_call_target="tpu_custom_call" | custom-call | flops 1073741824 | tf_op jit(solution)/shard_map/fetch/pallas_call | solution.py:32
  59.7 4.6 %channel_mixer.1 = (bf16[16,8,2048]{2,1,0:T(8,128)(2,1)S(1)}, f32[16,8,2048]{2,1,0:T(8,128)S(1)}, f32[8,2048]{1,0:T(8,128)S(1)}) custom-call(bf16[16,128,128]{2,1,0:T(8,128)(2,1)S(1)} %all_to_all.27.after_ref.own_ref, bf16[16,128,128]{2,1,0:T(8,128)(2,1)S(1)} %collective-permute-done.2.far_ref, f32[1,4096]{1,0:T(1,128)S(1)} %bitcast.17, ...), custom_call_target="tpu_custom_call" | custom-call | flops 1073741824 | tf_op jit(solution)/shard_map/channel_mixer/pallas_call | solution.py:32
  64.3 0.1 collective-permute-start.3
  64.4 1.9 %collective-permute-done.3.arrived_ref = bf16[16,8,2048]{2,1,0:T(8,128)(2,1)S(1)} collective-permute-done((bf16[16,8,2048]{2,1,0:T(8,128)(2,1)S(1)}, bf16[16,8,2048]{2,1,0:T(8,128)(2,1)S(1)}, u32[]{:S(2)}, u32[]{:S(2)}) %collective-permute-start.3) | collective-permute-done | bytes 524320 | tf_op jit(solution)/shard_map/ppermute | solution.py:23
  66.4 13.6 %all_to_all.28.arrived_ref = bf16[16,8,2048]{2,1,0:T(8,128)(2,1)S(1)} all-to-all(bf16[16,8,2048]{2,1,0:T(8,128)(2,1)S(1)} %add_terms.3), channel_id=1, replica_groups=mesh['dp'=4,'kv'=16,'tp'=2] {'kv'}, dimensions={0} | all-to-all | bytes 1048576 | tf_op jit(solution)/shard_map/all_to_all | solution.py:27
  80.0 1.0 %last_norm.1 = bf16[32,4,128]{2,1,0:T(4,128)(2,1)} custom-call(bf16[16,8,2048]{2,1,0:T(8,128)(2,1)S(1)} %all_to_all.28.arrived_ref, f32[8,2048]{1,0:T(8,128)S(1)} %get-tuple-element.26.row_ref, f32[1,4096]{1,0:T(1,128)S(1)} %bitcast.18), custom_call_target="tpu_custom_call" | custom-call | flops 1048576 | tf_op jit(solution)/shard_map/last_norm/pallas_call | solution.py:32
  81.0 5.1 %all-to-all-start.4 = ((bf16[32,4,128]{2,1,0:T(4,128)(2,1)}), bf16[32,4,128]{2,1,0:T(4,128)(2,1)S(1)}, u32[]{:S(2)}, u32[]{:S(2)}) async-start(bf16[32,4,128]{2,1,0:T(4,128)(2,1)} %last_norm.1), calls=%async_computation.4 | async-start | bytes 65536 | tf_op jit(solution)/shard_map/all_to_all | solution.py:27
  86.1 5.1 %next_state.1 = f32[8192,128]{1,0:T(8,128)} custom-call(f32[8192,128]{1,0:T(8,128)} %bitcast.21, f32[4,2048]{1,0:T(4,128)S(1)} %get-tuple-element.27.decay_ref, f32[4,2048]{1,0:T(4,128)S(1)} %get-tuple-element.28.drive_ref, f32[4,256]{1,0:T(4,128)S(1)} %get-tuple-element.29.write_ref), custom_call_target="tpu_custom_call" | custom-call | flops 1073741824 | tf_op jit(solution)/shard_map/next_state/pallas_call | solution.py:32
  91.2 2.3 %all-to-all-done.4 = bf16[32,4,128]{2,1,0:T(4,128)(2,1)S(1)} async-done(((bf16[32,4,128]{2,1,0:T(4,128)(2,1)}), bf16[32,4,128]{2,1,0:T(4,128)(2,1)S(1)}, u32[]{:S(2)}, u32[]{:S(2)}) %all-to-all-start.4) | async-done | bytes 32800 | tf_op jit(solution)/shard_map/all_to_all | solution.py:27
  93.5 0.6 copy.25
  (13 shorter events, 0.2 us)
Async XLA Ops:
  0.6 40.2 %copy-start = (bf16[2048,128]{1,0:T(8,128)(2,1)S(1)}, bf16[2048,128]{1,0:T(8,128)(2,1)}, u32[]{:S(2)}) copy-start(bf16[2048,128]{1,0:T(8,128)(2,1)} %param.39) | copy-start | bytes 1572868
  2.8 24.1 %copy-start.3 = (f32[2048]{0:T(1024)S(1)}, f32[2048]{0:T(1024)}, u32[]{:S(2)}) copy-start(f32[2048]{0:T(1024)} %param.38) | copy-start | bytes 24580
  2.8 3.9 %collective-permute-start = (bf16[16,8,2432]{2,1,0:T(8,128)(2,1)S(1)}, bf16[16,8,2432]{2,1,0:T(8,128)(2,1)S(1)}, u32[]{:S(2)}, u32[]{:S(2)}) collective-permute-start(bf16[16,8,2432]{2,1,0:T(8,128)(2,1)S(1)} %get-tuple-element.18), channel_id=1, source_target_pairs={{0,1},{1,0},{2,3},{3,2},{4,5},{5,4},{6,7},{7,6},{8,9},{9,8},{10,11... | collective-permute-start | bytes 1867784 | tf_op jit(solution)/shard_map/ppermute | solution.py:23
  38.3 3.6 %collective-permute-start.1 = (bf16[64,2048]{1,0:T(8,128)(2,1)S(1)}, bf16[64,2048]{1,0:T(8,128)(2,1)S(1)}, u32[]{:S(2)}, u32[]{:S(2)}) collective-permute-start(bf16[64,2048]{1,0:T(8,128)(2,1)S(1)} %reshape.17), channel_id=1, source_target_pairs={{0,1},{1,0},{2,3},{3,2},{4,5},{5,4},{6,7},{7,6},{8,9},{9,8},{10,11... | collective-permute-start | bytes 786440 | tf_op jit(solution)/shard_map/ppermute | solution.py:23
  55.7 4.0 %copy-start.1 = (f32[4096]{0:T(1024)S(1)}, f32[4096]{0:T(1024)}, u32[]{:S(2)}) copy-start(f32[4096]{0:T(1024)} %param.40) | copy-start | bytes 49156
  55.7 4.0 %collective-permute-start.2 = (bf16[16,128,128]{2,1,0:T(8,128)(2,1)S(1)}, bf16[16,128,128]{2,1,0:T(8,128)(2,1)S(1)}, u32[]{:S(2)}, u32[]{:S(2)}) collective-permute-start(bf16[16,128,128]{2,1,0:T(8,128)(2,1)S(1)} %all_to_all.27.after_ref.own_ref), channel_id=1, source_target_pairs={{0,1},{1,0},{2,3},{3,2},{4,5},{5,4},{6,7},{7,6},{8,9},{9,8},{10,11... | collective-permute-start | bytes 1572872 | tf_op jit(solution)/shard_map/ppermute | solution.py:23
  59.7 20.3 %copy-start.2 = (f32[4096]{0:T(1024)S(1)}, f32[4096]{0:T(1024)}, u32[]{:S(2)}) copy-start(f32[4096]{0:T(1024)} %param.43) | copy-start | bytes 49156
  64.3 2.0 %collective-permute-start.3 = (bf16[16,8,2048]{2,1,0:T(8,128)(2,1)S(1)}, bf16[16,8,2048]{2,1,0:T(8,128)(2,1)S(1)}, u32[]{:S(2)}, u32[]{:S(2)}) collective-permute-start(bf16[16,8,2048]{2,1,0:T(8,128)(2,1)S(1)} %get-tuple-element.25), channel_id=1, source_target_pairs={{0,1},{1,0},{2,3},{3,2},{4,5},{5,4},{6,7},{7,6},{8,9},{9,8},{10,11... | collective-permute-start | bytes 1572872 | tf_op jit(solution)/shard_map/ppermute | solution.py:23
  81.0 12.4 %all-to-all-start.4 = ((bf16[32,4,128]{2,1,0:T(4,128)(2,1)}), bf16[32,4,128]{2,1,0:T(4,128)(2,1)S(1)}, u32[]{:S(2)}, u32[]{:S(2)}) async-start(bf16[32,4,128]{2,1,0:T(4,128)(2,1)} %last_norm.1), calls=%async_computation.4 | async-start | bytes 65536 | tf_op jit(solution)/shard_map/all_to_all | solution.py:27

commit v3 on v2

--- a/solution.py
+++ b/solution.py
@@ -27,7 +27,7 @@
     return lax.all_to_all(parts, axis, split_axis=0, concat_axis=0, tiled=True)
 
 
-def kernel(body, outs, args, out_space=pltpu.VMEM, in_spaces=None, scratch=(), flops=0, limit=24):
+def kernel(body, outs, args, out_space=pltpu.VMEM, in_spaces=None, scratch=(), flops=0, limit=12):
     in_spaces = in_spaces or [pltpu.VMEM] * len(args)
     return pl.pallas_call(
         body,
@@ -46,7 +46,7 @@
 
 
 def sigmoid(value):
-    return 1.0 / (1.0 + jnp.exp(-value))
+    return lax.logistic(value)
 
 
 def upper_rows(shape):
@@ -69,7 +69,6 @@
     step_hbm,
     far_ref,
     own_ref,
-    order_ref,
     x_ref,
     gate_ref,
     value_ref,
@@ -95,12 +94,7 @@
         copy.start()
     copies[0].wait()
     rows_ref[0] = x_ref[...].astype(F32)
-    half = order_ref.shape[0] // 2
     for k in range(x_ref.shape[0] // 8):
-        for c in range(2):
-            order_ref[c * half + 4 * k : c * half + 4 * k + 4, :] = (
-                RESIDUAL_SCALE * rows_ref[0, 8 * k + 4 * c : 8 * k + 4 * c + 4, :]
-            )
         own = rows_ref[0, pl.ds(8 * k + 4 * core, 4), :]
         far = rows_ref[0, pl.ds(8 * k + 4 * (1 - core), 4), :]
         for place, value in ((1, own), (2, far)):
@@ -227,23 +221,48 @@
         state_ref[at, :] = states_ref[at, :].astype(BF16)
 
 
-def fetch(after_ref, up_hbm, up_ref, arrivals):
-    pieces = arrivals.shape[0]
-    rows = up_hbm.shape[0] // pieces
-    copies = []
-    for n in range(pieces):
-        at = pl.ds(n * rows, rows)
-        copies.append(pltpu.make_async_copy(up_hbm.at[at], up_ref.at[at], arrivals.at[n]))
-        copies[-1].start()
-    for copy in copies:
-        copy.wait()
+def mix_out(mixed_ref, own_weight_ref, far_weight_ref, own_input_ref, far_input_ref, out_ref, rows_ref):
+    core = lax.axis_index("tp")
+    lanes = own_input_ref.shape[1]
+    group = mixed_ref.shape[2]
+    half = out_ref.shape[1]
+    rows_ref[0] = own_input_ref[...].astype(F32)
+    rows_ref[1] = far_input_ref[...].astype(F32)
+    for k in range(half // 4):
+        for n in range(2):
+            rows_ref[2 + n, 4 * k : 4 * k + 4, :] = rows_ref[n, pl.ds(8 * k + 4 * core, 4), :]
+    mixed = mixed_ref[...].reshape(2 * half, group)
+    upper = upper_rows((half, lanes))
+    parts = []
+    for n, weight_ref in enumerate((own_weight_ref, far_weight_ref)):
+        first = dot(mixed, weight_ref[:group, :])
+        second = dot(mixed, weight_ref[group:, :])
+        both = (first + pltpu.roll(second, 2 * half - 4, 0)).reshape(half // 8, 16, lanes)
+        even = both[:, :8].reshape(half, lanes)
+        odd = both[:, 8:].reshape(half, lanes)
+        total = jnp.where(upper, even, pltpu.roll(odd, 4, 0))
+        parts.append((RESIDUAL_SCALE * rows_ref[2 + n, :half] + total).astype(BF16))
+    first = jnp.where(core == 0, parts[0], parts[1])
+    second = jnp.where(core == 0, parts[1], parts[0])
+    for k in range(out_ref.shape[0]):
+        out_ref[k, :, :lanes] = first
+        out_ref[k, :, lanes:] = second
 
 
 def mix(
-    arrived_ref, past_ref, taps_ref, head_ref, gain_ref, state_ref, out_ref, decay_ref, drive_ref, write_ref
+    arrived_ref,
+    past_ref,
+    taps_ref,
+    head_ref,
+    gain_ref,
+    state_ref,
+    out_ref,
+    decay_ref,
+    drive_ref,
+    write_ref,
 ):
     inner = gain_ref.shape[1]
-    seqs = out_ref.shape[1]
+    seqs = out_ref.shape[1] // GROUPS
     group = inner // GROUPS
     span = GROUPS * STATE_DIM
     total = total_of(arrived_ref).astype(BF16).astype(F32)
@@ -287,7 +306,8 @@
         cut = gated[:, g * group : (g + 1) * group]
         mean = jnp.sum(cut * cut, 1, keepdims=True) * (1.0 / group)
         normed.append(cut * lax.rsqrt(mean + MIXER_EPSILON))
-    mixed = (jnp.concatenate(normed, 1) * gain_ref[...]).astype(BF16)
+    mixed = [normed[g] * gain_ref[:, g * group : (g + 1) * group] for g in range(GROUPS)]
+    mixed = jnp.concatenate(mixed, 0).astype(BF16)
     for k in range(out_ref.shape[0]):
         out_ref[k] = mixed
     decay_ref[...] = decay
@@ -343,67 +363,50 @@
 
 
 def channel_mixer(
-    own_ref,
-    far_ref,
+    cols_ref,
     gain_ref,
-    up_ref,
-    down_hbm,
-    far_out_ref,
-    own_out_ref,
+    up_own_ref,
+    up_far_ref,
+    down_own_ref,
+    down_far_ref,
+    out_ref,
     row_ref,
     normed_ref,
-    down_ref,
-    arrivals,
 ):
-    pieces = arrivals.shape[0]
-    span = down_hbm.shape[0] // pieces
-    copies = []
-    for n in range(pieces):
-        at = pl.ds(n * span, span)
-        copies.append(pltpu.make_async_copy(down_hbm.at[at], down_ref.at[at], arrivals.at[n]))
-        copies[-1].start()
-    core = lax.axis_index("tp")
     chip = lax.axis_index("kv")
-    chips, rows_all, lanes = own_ref.shape
-    half = rows_all // 2
-    width = 2 * chips * lanes
-    total = jnp.zeros((rows_all, lanes), F32)
+    chips, half, lanes = cols_ref.shape
+    width = chips * lanes
+    total = jnp.zeros((half, lanes), F32)
     for k in range(chips):
-        total = total + own_ref[k].astype(F32) + far_ref[k].astype(F32)
+        total = total + cols_ref[k].astype(F32)
     mean = jnp.sum(total, 1, keepdims=True) * (1.0 / width)
-    square = jnp.zeros((rows_all, lanes), F32)
+    square = jnp.zeros((half, lanes), F32)
     for k in range(chips):
-        a = own_ref[k].astype(F32) - mean
-        b = far_ref[k].astype(F32) - mean
-        square = square + a * a + b * b
+        a = cols_ref[k].astype(F32) - mean
+        square = square + a * a
     scale = lax.rsqrt(jnp.sum(square, 1, keepdims=True) * (1.0 / width) + NORM_EPSILON)
     for k in range(chips):
-        own = own_ref[k].astype(F32)
-        far = far_ref[k].astype(F32)
-        pair = (jnp.where(core == 0, own, far), jnp.where(core == 0, far, own))
-        for c in range(2):
-            at = slice((2 * k + c) * lanes, (2 * k + c + 1) * lanes)
-            normed_ref[:, at] = ((pair[c] - mean) * scale * gain_ref[:, at]).astype(BF16)
-    hidden = jnp.maximum(dot(normed_ref[...], up_ref[...]), 0.0)
-    hidden = (hidden * hidden).astype(BF16)
-    for copy in copies:
-        copy.wait()
+        at = slice(k * lanes, (k + 1) * lanes)
+        centred = cols_ref[k].astype(F32) - mean
+        normed_ref[:, at] = (centred * scale * gain_ref[:, at]).astype(BF16)
+    hidden = []
+    for weight_ref in (up_own_ref, up_far_ref):
+        active = jnp.maximum(dot(normed_ref[...], weight_ref[...]), 0.0)
+        hidden.append((active * active).astype(BF16))
     chunk = 256
     upper = upper_rows((half, chunk))
     for n in range(width // 2 // chunk):
         at = slice(n * chunk, (n + 1) * chunk)
-        first = dot(hidden, down_ref[:, at])
-        second = dot(hidden, down_ref[:, width // 2 + n * chunk : width // 2 + (n + 1) * chunk])
-        for out_ref, here in ((far_out_ref, core == 1), (own_out_ref, core == 0)):
-            a = jnp.where(here, first[:half], first[half:])
-            b = jnp.where(here, second[:half], second[half:])
-            even = jnp.where(upper, a, pltpu.roll(b, 4, 0)).astype(out_ref.dtype)
-            odd = jnp.where(upper, pltpu.roll(a, half - 4, 0), b).astype(out_ref.dtype)
-            for r in range(half // 8):
-                out_ref[2 * r, :, at] = even[8 * r : 8 * r + 8]
-                out_ref[2 * r + 1, :, at] = odd[8 * r : 8 * r + 8]
-    shape = (8, rows_all)
-    wanted = core * half + chip * 4 + lax.broadcasted_iota(jnp.int32, shape, 0) % 4
+        past = slice(width // 2 + n * chunk, width // 2 + (n + 1) * chunk)
+        a = dot(hidden[0], down_own_ref[:, at]) + dot(hidden[1], down_far_ref[:, at])
+        b = dot(hidden[0], down_own_ref[:, past]) + dot(hidden[1], down_far_ref[:, past])
+        even = jnp.where(upper, a, pltpu.roll(b, 4, 0)).astype(out_ref.dtype)
+        odd = jnp.where(upper, pltpu.roll(a, half - 4, 0), b).astype(out_ref.dtype)
+        for r in range(half // 8):
+            out_ref[2 * r, :, at] = even[8 * r : 8 * r + 8]
+            out_ref[2 * r + 1, :, at] = odd[8 * r : 8 * r + 8]
+    shape = (8, half)
+    wanted = chip * 4 + lax.broadcasted_iota(jnp.int32, shape, 0) % 4
     pick = wanted == lax.broadcasted_iota(jnp.int32, shape, 1)
     rows = dot(pick.astype(F32).astype(BF16), normed_ref[...])
     row_ref[...] = jnp.where(
@@ -454,7 +457,6 @@
     down_weight,
     norm2_gain,
 ):
-    core = lax.axis_index("tp")
     chips = lax.axis_size("kv")
     width = norm1_gain.shape[0]
     inner = mixer_gain.shape[0]
@@ -464,9 +466,9 @@
 
     span = GROUPS * STATE_DIM
     terms_width = inner + span + LANES
-    far_terms, own_terms, scaled_input = kernel(
+    far_terms, own_terms = kernel(
         project_rows,
-        [((chips, 8, terms_width), BF16), ((chips, 8, terms_width), F32), (layer_input.shape, F32)],
+        [((chips, 8, terms_width), BF16), ((chips, 8, terms_width), F32)],
         [layer_input, gate_weight, value_weight, write_weight, read_weight, step_weight.T],
         in_spaces=[pltpu.HBM] * 6,
         scratch=[
@@ -508,11 +510,16 @@
     (terms,) = kernel(
         add_terms, [((chips, 8, terms_width), BF16)], [own_terms, arrived, taps], flops=2**20
     )
+    terms, far_input, far_out, up_from, down_from = lax.optimization_barrier(
+        (terms, other_core(layer_input), other_core(out_weight), up_weight, down_weight)
+    )
+    swapped = [other_core(weight) for weight in (up_from, down_from)]
     arrived = exchange(terms, "kv")
+    arrived, far_up, far_down = lax.optimization_barrier((arrived, *swapped))
     mixed, decay, drive, writes = kernel(
         mix,
         [
-            ((chips, rows, inner), BF16),
+            ((chips, GROUPS * rows, inner // GROUPS), BF16),
             ((rows, inner), F32),
             ((rows, inner), F32),
             ((rows, span), F32),
@@ -520,8 +527,7 @@
         [arrived, past, taps, heads, mixer_gain[None], states],
         flops=2**28,
     )
-    own_mixed = exchange(mixed, "kv").reshape(half, inner)
-    far_mixed = other_core(own_mixed)
+    mixed = exchange(mixed, "kv")
 
     (state_next,) = kernel(
         next_state,
@@ -539,37 +545,20 @@
     )
     state_next = state_next.reshape(state_past.shape)
 
-    own_mix, far_mix = dot(own_mixed, out_weight), dot(far_mixed, out_weight)
-    mix_out = jnp.concatenate(
-        [jnp.where(core == 0, own_mix, far_mix), jnp.where(core == 0, far_mix, own_mix)], 0
-    )
-    residual = (scaled_input + mix_out).astype(BF16)
-    own_columns = exchange(jnp.broadcast_to(residual, (chips, *residual.shape)), "kv")
-    far_columns = other_core(own_columns)
-    (up_here,) = kernel(
-        fetch,
-        [(up_weight.shape, BF16)],
-        [own_columns, up_weight],
-        in_spaces=[pltpu.VMEM, pltpu.HBM],
-        scratch=[pltpu.SemaphoreType.DMA((8,))],
-        flops=2**30,
-        limit=4,
-    )
-    far_terms, own_terms, normed_rows = kernel(
+    (columns,) = kernel(
+        mix_out,
+        [((chips, half, 2 * LANES), BF16)],
+        [mixed, out_weight, far_out, layer_input, far_input],
+        scratch=[pltpu.VMEM((4, 2 * half, LANES), F32)],
+        flops=2**28,
+    )
+    columns = exchange(columns, "kv")
+    terms, normed_rows = kernel(
         channel_mixer,
-        [((chips, 8, width // 2), BF16), ((chips, 8, width // 2), F32), ((8, width // 2), F32)],
-        [own_columns, far_columns, norm1_gain[None], up_here, down_weight],
-        in_spaces=[pltpu.VMEM] * 4 + [pltpu.HBM],
-        scratch=[
-            pltpu.VMEM((2 * half, width), BF16),
-            pltpu.VMEM(down_weight.shape, BF16),
-            pltpu.SemaphoreType.DMA((4,)),
-        ],
-        flops=2**30,
-    )
-    arrived = other_core(far_terms)
-    (terms,) = kernel(
-        add_terms, [((chips, 8, width // 2), BF16)], [own_terms, arrived], flops=2**20
+        [((chips, 8, width // 2), BF16), ((8, width // 2), F32)],
+        [columns, norm1_gain[None], up_weight, far_up, down_weight, far_down],
+        scratch=[pltpu.VMEM((half, width), BF16)],
+        flops=2**31,
     )
     arrived = exchange(terms, "kv")
     (result,) = kernel(

time: 94.4 us -> 85 us (0.900)
  Pallas kernels: 18.5 us -> 15.6 us
  blocking collectives: 57.6 us -> 54.7 us
  waiting for transfers between devices: 5.11 us -> 2.29 us
    ppermute x4 -> x5, starting transfers between devices: 5.8 us -> 2.56 us  [other_core(): return lax.ppermute(value, 'tp', SWAP)]
    all_to_all x1, starting transfers between devices: 5.07 us -> 8.11 us  [exchange(): return lax.all_to_all(parts, axis, split_axis=0, concat_axis=0, tiled=True)]
    all_to_all x4, blocking collectives: 57.6 us -> 54.7 us  [exchange(): return lax.all_to_all(parts, axis, split_axis=0, concat_axis=0, tiled=True)]
    pallas_call x9 -> x8, Pallas kernels: 18.5 us -> 15.6 us  [kernel(): pl.pallas_call(body, name=body.__name__, in_specs=[pl.BlockSpec(memory_sp...]
    ppermute x4 -> x5, waiting for transfers between devices: 2.83 us -> 0.01 us  [other_core(): return lax.ppermute(value, 'tp', SWAP)]
  transfers between devices with their start and end apart: 5 -> 6, of which waited for: 3 -> 1; matrix products, arithmetic and copies ran while one was open for 0% -> 0% of each run, Pallas kernels for 10% -> 9%
where the time goes in v3:
time: 85 us; the launch traced here: 84.7 us
  blocking collectives  54.7 us (64%)
  Pallas kernels  15.6 us (18%)
  starting transfers between devices  10.7 us (13%)
  waiting for transfers between devices  2.29 us (3%)
    all_to_all x4, blocking collectives, exchange(): return lax.all_to_all(parts, axis, split_axis=0, concat_axis=0, tiled=True)  54.7 us
    pallas_call x8, Pallas kernels, kernel(): pl.pallas_call(body, name=body.__name__, in_specs=[pl.BlockSpec(memory_sp...  15.6 us
    all_to_all x1, starting transfers between devices, exchange(): return lax.all_to_all(parts, axis, split_axis=0, concat_axis=0, tiled=True)  8.11 us
    ppermute x5, starting transfers between devices, other_core(): return lax.ppermute(value, 'tp', SWAP)  2.56 us
    all_to_all x1, waiting for transfers between devices, exchange(): return lax.all_to_all(parts, axis, split_axis=0, concat_axis=0, tiled=True)  2.27 us
  transfers between devices with their start and end apart: 6, of which 1 were waited for; matrix products, arithmetic and copies ran while one was open for 0% of the time, Pallas kernels for 9%

profile of v3, /device:TPU:1, one launch (start us, length us, event | category | flops | bytes accessed | tf_op | source)
XLA Modules:
  0.0 84.7 jit_solution(5458587038438721444)
XLA Ops:
  0.6 2.2 %project_rows.1 = (bf16[16,8,2432]{2,1,0:T(8,128)(2,1)S(1)}, f32[16,8,2432]{2,1,0:T(8,128)S(1)}) custom-call(bf16[128,128]{1,0:T(8,128)(2,1)} %own_input_ref.1, bf16[128,2048]{1,0:T(8,128)(2,1)} %gate_hbm.1, bf16[128,2048]{1,0:T(8,128)(2,1)} %value_hbm.1, bf16[128,256]{1,0:T(8,128)(2,1)} %write_hbm.1, bf16[128,256]{1,0:T(8,128)(2,1)} %read_hbm.1, ...), custom_call_target="tpu_custom_call" | custom-call | flops 268435456 | tf_op jit(solution)/shard_map/project_rows/pallas_call | solution.py:32
  2.8 0.0 copy-start.6
  2.9 1.5 %collective-permute-start = (bf16[16,8,2432]{2,1,0:T(8,128)(2,1)S(1)}, bf16[16,8,2432]{2,1,0:T(8,128)(2,1)S(1)}, u32[]{:S(2)}, u32[]{:S(2)}) collective-permute-start(bf16[16,8,2432]{2,1,0:T(8,128)(2,1)S(1)} %get-tuple-element.23), channel_id=1, source_target_pairs={{0,1},{1,0},{2,3},{3,2},{4,5},{5,4},{6,7},{7,6},{8,9},{9,8},{10,11... | collective-permute-start | bytes 1867784 | tf_op jit(solution)/shard_map/ppermute | solution.py:23
  4.3 0.1 collective-permute-start.2
  4.4 0.4 collective-permute-start.1
  4.8 2.4 %prepare.1 = (bf16[8192,128]{1,0:T(8,128)(2,1)S(1)}, f32[4,2560]{1,0:T(4,128)S(1)}, f32[1,2560]{1,0:T(1,128)S(1)}, f32[3,2048]{1,0:T(4,128)S(1)}) custom-call(f32[8192,128]{1,0:T(8,128)} %bitcast.16, bf16[3,4,2048]{2,1,0:T(4,128)(2,1)} %bitcast.20, bf16[3,4,256]{2,1,0:T(4,128)(2,1)} %bitcast.22, bf16[3,4,256]{2,1,0:T(4,128)(2,1)} %bitcast.23, ...), custom_call_target="tpu_custom_call" | custom-call | flops 536870912 | tf_op jit(solution)/shard_map/prepare/pallas_call | solution.py:32
  7.3 0.0 copy-start.2
  7.3 0.0 copy-start.3
  7.3 0.1 add_terms.1
  7.4 0.0 copy-start.1
  7.5 0.2 collective-permute-start.3
  7.6 0.4 collective-permute-start.4
  8.1 20.1 %all_to_all.25.arrived_ref = bf16[16,8,2432]{2,1,0:T(8,128)(2,1)S(1)} all-to-all(bf16[16,8,2432]{2,1,0:T(8,128)(2,1)S(1)} %add_terms.1), channel_id=1, replica_groups=mesh['dp'=4,'kv'=16,'tp'=2] {'kv'}, dimensions={0} | all-to-all | bytes 1245184 | tf_op jit(solution)/shard_map/all_to_all | solution.py:27
  28.2 0.8 mix.1
  29.0 10.6 %all_to_all.26.mixed_ref = bf16[16,8,1024]{2,1,0:T(8,128)(2,1)S(1)} all-to-all(bf16[16,8,1024]{2,1,0:T(8,128)(2,1)S(1)} %get-tuple-element.32), channel_id=1, replica_groups=mesh['dp'=4,'kv'=16,'tp'=2] {'kv'}, dimensions={0} | all-to-all | bytes 524288 | tf_op jit(solution)/shard_map/all_to_all | solution.py:27
  39.7 0.5 mix_out.1
  40.2 12.2 %all_to_all.27.cols_ref = bf16[16,64,256]{2,1,0:T(8,128)(2,1)S(1)} all-to-all(bf16[16,64,256]{2,1,0:T(8,128)(2,1)S(1)} %mix_out.1), channel_id=1, replica_groups=mesh['dp'=4,'kv'=16,'tp'=2] {'kv'}, dimensions={0} | all-to-all | bytes 1048576 | tf_op jit(solution)/shard_map/all_to_all | solution.py:27
  52.4 3.5 %channel_mixer.1 = (bf16[16,8,2048]{2,1,0:T(8,128)(2,1)S(1)}, f32[8,2048]{1,0:T(8,128)S(1)}) custom-call(bf16[16,64,256]{2,1,0:T(8,128)(2,1)S(1)} %all_to_all.27.cols_ref, f32[1,4096]{1,0:T(1,128)S(1)} %bitcast.13, bf16[4096,512]{1,0:T(8,128)(2,1)S(1)} %copy-done, bf16[4096,512]{1,0:T(8,128)(2,1)S(1)} %collective-permute-done.3.up_far_ref, ...), custom_call_target="tpu_custom_call" | custom-call | flops 2147483648 | tf_op jit(solution)/shard_map/channel_mixer/pallas_call | solution.py:32
  55.8 11.8 %all_to_all.28.arrived_ref = bf16[16,8,2048]{2,1,0:T(8,128)(2,1)S(1)} all-to-all(bf16[16,8,2048]{2,1,0:T(8,128)(2,1)S(1)} %get-tuple-element.37), channel_id=1, replica_groups=mesh['dp'=4,'kv'=16,'tp'=2] {'kv'}, dimensions={0} | all-to-all | bytes 1048576 | tf_op jit(solution)/shard_map/all_to_all | solution.py:27
  67.6 1.0 %last_norm.1 = bf16[32,4,128]{2,1,0:T(4,128)(2,1)} custom-call(bf16[16,8,2048]{2,1,0:T(8,128)(2,1)S(1)} %all_to_all.28.arrived_ref, f32[8,2048]{1,0:T(8,128)S(1)} %get-tuple-element.38.row_ref, f32[1,4096]{1,0:T(1,128)S(1)} %bitcast.14), custom_call_target="tpu_custom_call" | custom-call | flops 1048576 | tf_op jit(solution)/shard_map/last_norm/pallas_call | solution.py:32
  68.6 8.1 %all-to-all-start.4 = ((bf16[32,4,128]{2,1,0:T(4,128)(2,1)}), bf16[32,4,128]{2,1,0:T(4,128)(2,1)S(1)}, u32[]{:S(2)}, u32[]{:S(2)}) async-start(bf16[32,4,128]{2,1,0:T(4,128)(2,1)} %last_norm.1), calls=%async_computation.4 | async-start | bytes 65536 | tf_op jit(solution)/shard_map/all_to_all | solution.py:27
  76.7 5.1 %next_state.1 = f32[8192,128]{1,0:T(8,128)} custom-call(f32[8192,128]{1,0:T(8,128)} %bitcast.17, f32[4,2048]{1,0:T(4,128)S(1)} %get-tuple-element.39.decay_ref, f32[4,2048]{1,0:T(4,128)S(1)} %get-tuple-element.40.drive_ref, f32[4,256]{1,0:T(4,128)S(1)} %get-tuple-element.41.write_ref), custom_call_target="tpu_custom_call" | custom-call | flops 1073741824 | tf_op jit(solution)/shard_map/next_state/pallas_call | solution.py:32
  81.8 2.3 %all-to-all-done.4 = bf16[32,4,128]{2,1,0:T(4,128)(2,1)S(1)} async-done(((bf16[32,4,128]{2,1,0:T(4,128)(2,1)}), bf16[32,4,128]{2,1,0:T(4,128)(2,1)S(1)}, u32[]{:S(2)}, u32[]{:S(2)}) %all-to-all-start.4) | async-done | bytes 32800 | tf_op jit(solution)/shard_map/all_to_all | solution.py:27
  84.1 0.6 copy.25
  (15 shorter events, 0.0 us)
Async XLA Ops:
  0.6 6.8 %copy-start = (bf16[4096,512]{1,0:T(8,128)(2,1)S(1)}, bf16[4096,512]{1,0:T(8,128)(2,1)}, u32[]{:S(2)}) copy-start(bf16[4096,512]{1,0:T(8,128)(2,1)} %up_own_ref.1) | copy-start | bytes 12582916
  2.8 25.3 %copy-start.6 = (f32[2048]{0:T(1024)S(1)}, f32[2048]{0:T(1024)}, u32[]{:S(2)}) copy-start(f32[2048]{0:T(1024)} %param.38) | copy-start | bytes 24580
  2.9 4.4 %collective-permute-start = (bf16[16,8,2432]{2,1,0:T(8,128)(2,1)S(1)}, bf16[16,8,2432]{2,1,0:T(8,128)(2,1)S(1)}, u32[]{:S(2)}, u32[]{:S(2)}) collective-permute-start(bf16[16,8,2432]{2,1,0:T(8,128)(2,1)S(1)} %get-tuple-element.23), channel_id=1, source_target_pairs={{0,1},{1,0},{2,3},{3,2},{4,5},{5,4},{6,7},{7,6},{8,9},{9,8},{10,11... | collective-permute-start | bytes 1867784 | tf_op jit(solution)/shard_map/ppermute | solution.py:23
  4.3 3.1 %collective-permute-start.2 = (bf16[2048,128]{1,0:T(8,128)(2,1)}, bf16[2048,128]{1,0:T(8,128)(2,1)S(1)}, u32[]{:S(2)}, u32[]{:S(2)}) collective-permute-start(bf16[2048,128]{1,0:T(8,128)(2,1)} %own_weight_ref.1), channel_id=1, source_target_pairs={{0,1},{1,0},{2,3},{3,2},{4,5},{5,4},{6,7},{7,6},{8,9},{9,8},{10,11... | collective-permute-start | bytes 1572872 | tf_op jit(solution)/shard_map/ppermute | solution.py:23
  4.4 3.0 %collective-permute-start.1 = (bf16[128,128]{1,0:T(8,128)(2,1)}, bf16[128,128]{1,0:T(8,128)(2,1)S(1)}, u32[]{:S(2)}, u32[]{:S(2)}) collective-permute-start(bf16[128,128]{1,0:T(8,128)(2,1)} %own_input_ref.1), channel_id=1, source_target_pairs={{0,1},{1,0},{2,3},{3,2},{4,5},{5,4},{6,7},{7,6},{8,9},{9,8},{10,11... | collective-permute-start | bytes 98312 | tf_op jit(solution)/shard_map/ppermute | solution.py:23
  7.3 32.4 %copy-start.2 = (bf16[2048,128]{1,0:T(8,128)(2,1)S(1)}, bf16[2048,128]{1,0:T(8,128)(2,1)}, u32[]{:S(2)}) copy-start(bf16[2048,128]{1,0:T(8,128)(2,1)} %own_weight_ref.1) | copy-start | bytes 1572868
  7.3 32.4 %copy-start.3 = (bf16[128,128]{1,0:T(8,128)(2,1)S(1)}, bf16[128,128]{1,0:T(8,128)(2,1)}, u32[]{:S(2)}) copy-start(bf16[128,128]{1,0:T(8,128)(2,1)} %own_input_ref.1) | copy-start | bytes 98308
  7.4 44.9 %copy-start.1 = (bf16[512,4096]{1,0:T(8,128)(2,1)S(1)}, bf16[512,4096]{1,0:T(8,128)(2,1)}, u32[]{:S(2)}) copy-start(bf16[512,4096]{1,0:T(8,128)(2,1)} %down_own_ref.1) | copy-start | bytes 12582916
  7.4 44.9 %copy-start.4 = (f32[4096]{0:T(1024)S(1)}, f32[4096]{0:T(1024)}, u32[]{:S(2)}) copy-start(f32[4096]{0:T(1024)} %param.40) | copy-start | bytes 49156
  7.5 20.7 %collective-permute-start.3 = (bf16[4096,512]{1,0:T(8,128)(2,1)S(1)}, bf16[4096,512]{1,0:T(8,128)(2,1)S(1)}, u32[]{:S(2)}, u32[]{:S(2)}) collective-permute-start(bf16[4096,512]{1,0:T(8,128)(2,1)S(1)} %copy-done), channel_id=1, source_target_pairs={{0,1},{1,0},{2,3},{3,2},{4,5},{5,4},{6,7},{7,6},{8,9},{9,8},{10,11... | collective-permute-start | bytes 12582920 | tf_op jit(solution)/shard_map/ppermute | solution.py:23
  7.6 20.5 %collective-permute-start.4 = (bf16[512,4096]{1,0:T(8,128)(2,1)}, bf16[512,4096]{1,0:T(8,128)(2,1)S(1)}, u32[]{:S(2)}, u32[]{:S(2)}) collective-permute-start(bf16[512,4096]{1,0:T(8,128)(2,1)} %down_own_ref.1), channel_id=1, source_target_pairs={{0,1},{1,0},{2,3},{3,2},{4,5},{5,4},{6,7},{7,6},{8,9},{9,8},{10,11... | collective-permute-start | bytes 12582920 | tf_op jit(solution)/shard_map/ppermute | solution.py:23
  52.4 15.2 %copy-start.5 = (f32[4096]{0:T(1024)S(1)}, f32[4096]{0:T(1024)}, u32[]{:S(2)}) copy-start(f32[4096]{0:T(1024)} %param.43) | copy-start | bytes 49156
  68.6 15.5 %all-to-all-start.4 = ((bf16[32,4,128]{2,1,0:T(4,128)(2,1)}), bf16[32,4,128]{2,1,0:T(4,128)(2,1)S(1)}, u32[]{:S(2)}, u32[]{:S(2)}) async-start(bf16[32,4,128]{2,1,0:T(4,128)(2,1)} %last_norm.1), calls=%async_computation.4 | async-start | bytes 65536 | tf_op jit(solution)/shard_map/all_to_all | solution.py:27

commit v4 on v3

--- a/solution.py
+++ b/solution.py
@@ -27,14 +27,15 @@
     return lax.all_to_all(parts, axis, split_axis=0, concat_axis=0, tiled=True)
 
 
-def kernel(body, outs, args, out_space=pltpu.VMEM, in_spaces=None, scratch=(), flops=0, limit=12):
+def kernel(body, outs, args, out_spaces=None, in_spaces=None, scratch=(), flops=0, limit=12):
     in_spaces = in_spaces or [pltpu.VMEM] * len(args)
+    out_spaces = out_spaces or [pltpu.VMEM] * len(outs)
     return pl.pallas_call(
         body,
         name=body.__name__,
         in_specs=[pl.BlockSpec(memory_space=space) for space in in_spaces],
-        out_specs=[pl.BlockSpec(memory_space=out_space)] * len(outs),
-        out_shape=[out_space(shape, dtype) for shape, dtype in outs],
+        out_specs=[pl.BlockSpec(memory_space=space) for space in out_spaces],
+        out_shape=[space(*out) for space, out in zip(out_spaces, outs)],
         scratch_shapes=list(scratch),
         compiler_params=pltpu.CompilerParams(vmem_limit_bytes=limit * 2**20),
         cost_estimate=pl.CostEstimate(flops=flops, bytes_accessed=0, transcendentals=0),
@@ -110,7 +111,10 @@
     for rows, out_ref in ((far, far_ref), (own, own_ref)):
         steps = lax.dot_general(rows, step_ref[...], NT, preferred_element_type=F32)
         steps = jnp.where(upper_rows(steps.shape), steps, 0.0)
-        out_ref[:, :, inner + group :] = steps.astype(out_ref.dtype).reshape(-1, 8, LANES)
+        at = slice(inner + group, inner + group + LANES)
+        out_ref[:, :, at] = steps.astype(out_ref.dtype).reshape(-1, 8, LANES)
+        at = slice(inner + group + LANES, inner + group + 2 * LANES)
+        out_ref[:, :, at] = rows.astype(out_ref.dtype).reshape(-1, 8, LANES)
     copies[2].wait()
     copies[3].wait()
     for rows, out_ref in ((far, far_ref), (own, own_ref)):
@@ -128,10 +132,15 @@
             out_ref[:, :, at] = both.reshape(-1, 8, chunk)
 
 
-def add_terms(own_ref, arrived_ref, *rest):
-    out_ref = rest[-1]
+def add_terms(own_ref, arrived_ref, after_ref, out_ref, input_ref):
+    width = out_ref.shape[2] - LANES
     for k in range(out_ref.shape[0]):
-        out_ref[k] = (own_ref[k] + arrived_ref[k].astype(F32)).astype(BF16)
+        total = own_ref[k, :, :width] + arrived_ref[k, :, :width].astype(F32)
+        out_ref[k, :, :width] = total.astype(BF16)
+        out_ref[k, :, width:] = jnp.zeros((8, LANES), BF16)
+        for n, ref in enumerate((own_ref, arrived_ref)):
+            rows = ref[k, :, width:].astype(F32)
+            input_ref[n, 4 * k : 4 * k + 4, :] = RESIDUAL_SCALE * rows[:4]
 
 
 def spread_heads(rows, inner):
@@ -143,7 +152,6 @@
 
 
 def prepare(
-    state_hbm,
     past_value_hbm,
     past_write_hbm,
     past_read_hbm,
@@ -153,11 +161,9 @@
     bias_hbm,
     rate_hbm,
     skip_hbm,
-    state_ref,
     past_ref,
     taps_ref,
     head_ref,
-    states_ref,
     past_value_ref,
     past_write_ref,
     past_read_ref,
@@ -168,7 +174,6 @@
     rate_ref,
     skip_ref,
     arrivals,
-    state_arrivals,
 ):
     pairs = (
         (past_value_hbm, past_value_ref),
@@ -186,15 +191,6 @@
     ]
     for copy in copies:
         copy.start()
-    pieces = state_arrivals.shape[0]
-    rows = state_ref.shape[0] // pieces
-    state_copies = []
-    for n in range(pieces):
-        at = pl.ds(n * rows, rows)
-        state_copies.append(
-            pltpu.make_async_copy(state_hbm.at[at], states_ref.at[at], state_arrivals.at[n])
-        )
-        state_copies[-1].start()
     for copy in copies:
         copy.wait()
     at = 0
@@ -215,22 +211,13 @@
     terms = jnp.concatenate(split_terms(heads, 3), 0).astype(BF16)
     wide = spread_heads(terms, head_ref.shape[1])
     head_ref[...] = wide[0:3] + wide[3:6] + wide[6:9]
-    for n in range(pieces):
-        state_copies[n].wait()
-        at = slice(n * rows, (n + 1) * rows)
-        state_ref[at, :] = states_ref[at, :].astype(BF16)
-
-
-def mix_out(mixed_ref, own_weight_ref, far_weight_ref, own_input_ref, far_input_ref, out_ref, rows_ref):
+
+
+def mix_out(mixed_ref, own_weight_ref, far_weight_ref, input_ref, out_ref):
     core = lax.axis_index("tp")
-    lanes = own_input_ref.shape[1]
+    lanes = input_ref.shape[2]
     group = mixed_ref.shape[2]
     half = out_ref.shape[1]
-    rows_ref[0] = own_input_ref[...].astype(F32)
-    rows_ref[1] = far_input_ref[...].astype(F32)
-    for k in range(half // 4):
-        for n in range(2):
-            rows_ref[2 + n, 4 * k : 4 * k + 4, :] = rows_ref[n, pl.ds(8 * k + 4 * core, 4), :]
     mixed = mixed_ref[...].reshape(2 * half, group)
     upper = upper_rows((half, lanes))
     parts = []
@@ -241,7 +228,7 @@
         even = both[:, :8].reshape(half, lanes)
         odd = both[:, 8:].reshape(half, lanes)
         total = jnp.where(upper, even, pltpu.roll(odd, 4, 0))
-        parts.append((RESIDUAL_SCALE * rows_ref[2 + n, :half] + total).astype(BF16))
+        parts.append((input_ref[n] + total).astype(BF16))
     first = jnp.where(core == 0, parts[0], parts[1])
     second = jnp.where(core == 0, parts[1], parts[0])
     for k in range(out_ref.shape[0]):
@@ -290,7 +277,8 @@
         part = jnp.zeros((seqs, group), F32)
         for s in range(seqs):
             base = (s * GROUPS + g) * group
-            found = lax.dot_general(query, state_ref[base : base + group, :], NT, preferred_element_type=F32)
+            states = state_ref[base : base + group, :].astype(BF16)
+            found = lax.dot_general(query, states, NT, preferred_element_type=F32)
             part = jnp.where(row == s, found[:seqs] + found[seqs:], part)
         recalled.append(part)
         both = jnp.sum(writes[:, at] * reads[:, at], 1, keepdims=True)
@@ -323,45 +311,6 @@
     return terms
 
 
-def next_state(
-    state_hbm, decay_ref, drive_ref, write_ref, out_hbm, state_ref, out_ref, arrivals, departures
-):
-    seqs, inner = decay_ref.shape
-    group = inner // GROUPS
-    copies, loads = [], []
-    for n in range(seqs * GROUPS):
-        span = pl.ds(n * group, group)
-        loads.append(pltpu.make_async_copy(state_hbm.at[span], state_ref.at[span], arrivals.at[n]))
-        loads[-1].start()
-    for s in range(seqs):
-        for g in range(GROUPS):
-            at = slice(g * group, (g + 1) * group)
-            decay = split_terms(decay_ref[s : s + 1, at], 3)
-            drive = split_terms(drive_ref[s : s + 1, at], 2)
-            write = split_terms(write_ref[s : s + 1, g * STATE_DIM : (g + 1) * STATE_DIM], 2)
-            one = jnp.ones((1, STATE_DIM), F32)
-            blank_left, blank_right = jnp.zeros((5, group), F32), jnp.zeros((5, STATE_DIM), F32)
-            left = jnp.concatenate([*decay, blank_left], 0).T.astype(BF16)
-            right = jnp.concatenate([one, one, one, blank_right], 0).astype(BF16)
-            factor = dot(left, right)
-            left = jnp.concatenate([drive[0], drive[1], drive[0], blank_left], 0).T.astype(BF16)
-            right = jnp.concatenate([write[0], write[0], write[1], blank_right], 0).astype(BF16)
-            added = dot(left, right)
-            base = (s * GROUPS + g) * group
-            rows = slice(base, base + group)
-            loads[s * GROUPS + g].wait()
-            out_ref[rows, :] = factor * state_ref[rows, :] + added
-            span = pl.ds(base, group)
-            copies.append(
-                pltpu.make_async_copy(
-                    out_ref.at[span], out_hbm.at[span], departures.at[len(copies)]
-                )
-            )
-            copies[-1].start()
-    for copy in copies:
-        copy.wait()
-
-
 def channel_mixer(
     cols_ref,
     gain_ref,
@@ -369,10 +318,39 @@
     up_far_ref,
     down_own_ref,
     down_far_ref,
+    state_ref,
+    decay_ref,
+    drive_ref,
+    write_ref,
     out_ref,
     row_ref,
+    next_hbm,
     normed_ref,
+    side_ref,
+    next_ref,
+    departures,
 ):
+    seqs, inner = decay_ref.shape
+    group = inner // GROUPS
+    side_ref[...] = jnp.concatenate([decay_ref[...], drive_ref[...]], 0).T
+
+    def next_state(s, g):
+        base = (s * GROUPS + g) * group
+        write = write_ref[s : s + 1, g * STATE_DIM : (g + 1) * STATE_DIM]
+        for h in range(group // HEAD_DIM):
+            first = g * group + h * HEAD_DIM
+            drive = side_ref[first : first + HEAD_DIM, seqs + s : seqs + s + 1]
+            decay = jnp.broadcast_to(side_ref[first : first + 8, s : s + 1], (8, STATE_DIM))
+            rows = slice(base + h * HEAD_DIM, base + (h + 1) * HEAD_DIM)
+            kept = state_ref[rows, :].reshape(HEAD_DIM // 8, 8, STATE_DIM) * decay[None]
+            next_ref[rows, :] = kept.reshape(HEAD_DIM, STATE_DIM) + drive * write
+        at = pl.ds(base, group)
+        copy = pltpu.make_async_copy(
+            next_ref.at[at], next_hbm.at[at], departures.at[s * GROUPS + g]
+        )
+        copy.start()
+        return copy
+
     chip = lax.axis_index("kv")
     chips, half, lanes = cols_ref.shape
     width = chips * lanes
@@ -385,13 +363,20 @@
         a = cols_ref[k].astype(F32) - mean
         square = square + a * a
     scale = lax.rsqrt(jnp.sum(square, 1, keepdims=True) * (1.0 / width) + NORM_EPSILON)
+    sums = [jnp.zeros((half, up_own_ref.shape[1]), F32)] * 2
+    blocks = [(s, g) for s in range(seqs) for g in range(GROUPS)]
+    copies = []
     for k in range(chips):
+        if k % (chips // len(blocks)) == 0:
+            copies.append(next_state(*blocks[len(copies)]))
         at = slice(k * lanes, (k + 1) * lanes)
         centred = cols_ref[k].astype(F32) - mean
-        normed_ref[:, at] = (centred * scale * gain_ref[:, at]).astype(BF16)
+        rows = (centred * scale * gain_ref[:, at]).astype(BF16)
+        normed_ref[:, at] = rows
+        sums = [a + dot(rows, ref[at, :]) for a, ref in zip(sums, (up_own_ref, up_far_ref))]
     hidden = []
-    for weight_ref in (up_own_ref, up_far_ref):
-        active = jnp.maximum(dot(normed_ref[...], weight_ref[...]), 0.0)
+    for total in sums:
+        active = jnp.maximum(total, 0.0)
         hidden.append((active * active).astype(BF16))
     chunk = 256
     upper = upper_rows((half, chunk))
@@ -412,6 +397,8 @@
     row_ref[...] = jnp.where(
         upper_rows(row_ref.shape), rows[:, : width // 2], rows[:, width // 2 :]
     )
+    for copy in copies:
+        copy.wait()
 
 
 def last_norm(arrived_ref, row_ref, gain_ref, out_ref):
@@ -465,7 +452,7 @@
     per_head = inner // HEADS
 
     span = GROUPS * STATE_DIM
-    terms_width = inner + span + LANES
+    terms_width = inner + span + 2 * LANES
     far_terms, own_terms = kernel(
         project_rows,
         [((chips, 8, terms_width), BF16), ((chips, 8, terms_width), F32)],
@@ -489,29 +476,22 @@
     small += [value_taps, write_taps, read_taps]
     small += [step_bias[None], decay_log[None], skip_scale[None]]
     conv_width = inner + 2 * span
-    states, past, taps, heads = kernel(
+    past, taps, heads = kernel(
         prepare,
-        [
-            (state_rows.shape, BF16),
-            ((rows, conv_width), F32),
-            ((1, conv_width), F32),
-            ((3, inner), F32),
-        ],
-        [state_rows, *small],
-        in_spaces=[pltpu.HBM] * 10,
-        scratch=[
-            pltpu.VMEM(state_rows.shape, F32),
-            *[pltpu.VMEM(a.shape, a.dtype) for a in small],
-            pltpu.SemaphoreType.DMA((9,)),
-            pltpu.SemaphoreType.DMA((8,)),
-        ],
+        [((rows, conv_width), F32), ((1, conv_width), F32), ((3, inner), F32)],
+        small,
+        in_spaces=[pltpu.HBM] * 9,
+        scratch=[*[pltpu.VMEM(a.shape, a.dtype) for a in small], pltpu.SemaphoreType.DMA((9,))],
         flops=2**29,
     )
-    (terms,) = kernel(
-        add_terms, [((chips, 8, terms_width), BF16)], [own_terms, arrived, taps], flops=2**20
-    )
-    terms, far_input, far_out, up_from, down_from = lax.optimization_barrier(
-        (terms, other_core(layer_input), other_core(out_weight), up_weight, down_weight)
+    terms, inputs = kernel(
+        add_terms,
+        [((chips, 8, terms_width), BF16), ((2, half, LANES), F32)],
+        [own_terms, arrived, taps],
+        flops=2**20,
+    )
+    terms, far_out, up_from, down_from = lax.optimization_barrier(
+        (terms, other_core(out_weight), up_weight, down_weight)
     )
     swapped = [other_core(weight) for weight in (up_from, down_from)]
     arrived = exchange(terms, "kv")
@@ -524,40 +504,40 @@
             ((rows, inner), F32),
             ((rows, span), F32),
         ],
-        [arrived, past, taps, heads, mixer_gain[None], states],
+        [arrived, past, taps, heads, mixer_gain[None], state_rows],
         flops=2**28,
     )
     mixed = exchange(mixed, "kv")
-
-    (state_next,) = kernel(
-        next_state,
-        [(state_rows.shape, F32)],
-        [state_rows, decay, drive, writes],
-        in_spaces=[pltpu.HBM] + [pltpu.VMEM] * 3,
-        out_space=pltpu.HBM,
-        scratch=[
-            pltpu.VMEM(state_rows.shape, F32),
-            pltpu.VMEM(state_rows.shape, F32),
-            pltpu.SemaphoreType.DMA((8,)),
-            pltpu.SemaphoreType.DMA((8,)),
-        ],
-        flops=2**30,
-    )
-    state_next = state_next.reshape(state_past.shape)
 
     (columns,) = kernel(
         mix_out,
         [((chips, half, 2 * LANES), BF16)],
-        [mixed, out_weight, far_out, layer_input, far_input],
-        scratch=[pltpu.VMEM((4, 2 * half, LANES), F32)],
+        [mixed, out_weight, far_out, inputs],
         flops=2**28,
     )
     columns = exchange(columns, "kv")
-    terms, normed_rows = kernel(
+    terms, normed_rows, state_next = kernel(
         channel_mixer,
-        [((chips, 8, width // 2), BF16), ((8, width // 2), F32)],
-        [columns, norm1_gain[None], up_weight, far_up, down_weight, far_down],
-        scratch=[pltpu.VMEM((half, width), BF16)],
+        [((chips, 8, width // 2), BF16), ((8, width // 2), F32), (state_rows.shape, F32)],
+        [
+            columns,
+            norm1_gain[None],
+            up_weight,
+            far_up,
+            down_weight,
+            far_down,
+            state_rows,
+            decay,
+            drive,
+            writes,
+        ],
+        out_spaces=[pltpu.VMEM, pltpu.VMEM, pltpu.HBM],
+        scratch=[
+            pltpu.VMEM((half, width), BF16),
+            pltpu.VMEM((inner, 2 * rows), F32),
+            pltpu.VMEM(state_rows.shape, F32),
+            pltpu.SemaphoreType.DMA((8,)),
+        ],
         flops=2**31,
     )
     arrived = exchange(terms, "kv")
@@ -568,7 +548,7 @@
         flops=2**20,
     )
     result = exchange(result, ("kv", "tp")).reshape(2 * half, LANES)
-    return (result, state_next)
+    return (result, state_next.reshape(state_past.shape))
 
 
 def solution(mesh):

time: 85 us -> 84.3 us (level)
  blocking collectives: 54.7 us -> 70 us
  starting transfers between devices: 10.7 us -> 2.06 us
  Pallas kernels: 15.6 us -> 9.41 us
  waiting for transfers between devices: 2.29 us -> 1.14 us
    all_to_all x4 -> x5, blocking collectives: 54.7 us -> 70 us  [exchange(): return lax.all_to_all(parts, axis, split_axis=0, concat_axis=0, tiled=True)]
    all_to_all x1 -> x0, starting transfers between devices: 8.11 us -> none  [exchange(): return lax.all_to_all(parts, axis, split_axis=0, concat_axis=0, tiled=True)]
    pallas_call x8 -> x7, Pallas kernels: 15.6 us -> 9.41 us  [kernel(): pl.pallas_call(body, name=body.__name__, in_specs=[pl.BlockSpec(memory_sp...]
    all_to_all x1 -> x0, waiting for transfers between devices: 2.27 us -> none  [exchange(): return lax.all_to_all(parts, axis, split_axis=0, concat_axis=0, tiled=True)]
    ppermute x5 -> x4, waiting for transfers between devices: 0.01 us -> 1.14 us  [other_core(): return lax.ppermute(value, 'tp', SWAP)]
    ppermute x5 -> x4, starting transfers between devices: 2.56 us -> 2.06 us  [other_core(): return lax.ppermute(value, 'tp', SWAP)]
  transfers between devices with their start and end apart: 6 -> 4, of which waited for: 1 -> 2; matrix products, arithmetic and copies ran while one was open for 0% -> 0% of each run, Pallas kernels for 9% -> 1%
where the time goes in v4:
time: 84.3 us; the launch traced here: 84 us
  blocking collectives  70 us (83%)
  Pallas kernels  9.41 us (11%)
  starting transfers between devices  2.06 us (2%)
  waiting for transfers between devices  1.14 us (1%)
    all_to_all x5, blocking collectives, exchange(): return lax.all_to_all(parts, axis, split_axis=0, concat_axis=0, tiled=True)  70 us
    pallas_call x7, Pallas kernels, kernel(): pl.pallas_call(body, name=body.__name__, in_specs=[pl.BlockSpec(memory_sp...  9.41 us
    ppermute x4, starting transfers between devices, other_core(): return lax.ppermute(value, 'tp', SWAP)  2.06 us
  transfers between devices with their start and end apart: 4, of which 2 were waited for; matrix products, arithmetic and copies ran while one was open for 0% of the time, Pallas kernels for 1%

profile of v4, /device:TPU:1, one launch (start us, length us, event | category | flops | bytes accessed | tf_op | source)
XLA Modules:
  0.0 84.0 jit_solution(10527730820496038206)
XLA Ops:
  0.7 2.2 %project_rows.1 = (bf16[16,8,2560]{2,1,0:T(8,128)(2,1)S(1)}, f32[16,8,2560]{2,1,0:T(8,128)S(1)}) custom-call(bf16[128,128]{1,0:T(8,128)(2,1)} %x_hbm.1, bf16[128,2048]{1,0:T(8,128)(2,1)} %gate_hbm.1, bf16[128,2048]{1,0:T(8,128)(2,1)} %value_hbm.1, bf16[128,256]{1,0:T(8,128)(2,1)} %write_hbm.1, bf16[128,256]{1,0:T(8,128)(2,1)} %read_hbm.1, ...), custom_call_target="tpu_custom_call" | custom-call | flops 268435456 | tf_op jit(solution)/shard_map/project_rows/pallas_call | solution.py:33
  2.9 1.5 %collective-permute-start = (bf16[16,8,2560]{2,1,0:T(8,128)(2,1)S(1)}, bf16[16,8,2560]{2,1,0:T(8,128)(2,1)S(1)}, u32[]{:S(2)}, u32[]{:S(2)}) collective-permute-start(bf16[16,8,2560]{2,1,0:T(8,128)(2,1)S(1)} %get-tuple-element.24), channel_id=1, source_target_pairs={{0,1},{1,0},{2,3},{3,2},{4,5},{5,4},{6,7},{7,6},{8,9},{9,8},{10,11... | collective-permute-start | bytes 1966088 | tf_op jit(solution)/shard_map/ppermute | solution.py:23
  4.3 0.1 collective-permute-start.1
  4.4 1.1 %prepare.1 = (f32[4,2560]{1,0:T(4,128)S(1)}, f32[1,2560]{1,0:T(1,128)S(1)}, f32[3,2048]{1,0:T(4,128)S(1)}) custom-call(bf16[3,4,2048]{2,1,0:T(4,128)(2,1)} %bitcast.21, bf16[3,4,256]{2,1,0:T(4,128)(2,1)} %bitcast.22, bf16[3,4,256]{2,1,0:T(4,128)(2,1)} %bitcast.23, bf16[4,2048]{1,0:T(4,128)(2,1)} %value_taps_hbm.1, bf16[4,256]{1,0:T(4,128)(2,1)} %write_taps_hbm.1, ...), custom_call_target="tpu_custom_call" | custom-call | flops 536870912 | tf_op jit(solution)/shard_map/prepare/pallas_call | solution.py:33
  5.5 0.5 collective-permute-done.arrived_ref
  6.0 0.1 add_terms.1
  6.2 0.6 collective-permute-done.1.far_weight_ref
  6.8 0.4 collective-permute-start.2
  7.2 0.1 collective-permute-start.3
  7.3 20.1 %all_to_all.25.arrived_ref = bf16[16,8,2560]{2,1,0:T(8,128)(2,1)S(1)} all-to-all(bf16[16,8,2560]{2,1,0:T(8,128)(2,1)S(1)} %get-tuple-element.27), channel_id=1, replica_groups=mesh['dp'=4,'kv'=16,'tp'=2] {'kv'}, dimensions={0} | all-to-all | bytes 1310720 | tf_op jit(solution)/shard_map/all_to_all | solution.py:27
  27.4 0.0 collective-permute-done.3.down_far_ref
  27.4 0.0 copy-start.1
  27.4 0.0 copy-start.2
  27.4 0.0 copy-start.4
  27.5 0.9 %mix.1 = (bf16[16,8,1024]{2,1,0:T(8,128)(2,1)S(1)}, f32[4,2048]{1,0:T(4,128)S(1)}, f32[4,2048]{1,0:T(4,128)S(1)}, f32[4,256]{1,0:T(4,128)S(1)}) custom-call(bf16[16,8,2560]{2,1,0:T(8,128)(2,1)S(1)} %all_to_all.25.arrived_ref, f32[4,2560]{1,0:T(4,128)S(1)} %get-tuple-element.31.past_ref, f32[1,2560]{1,0:T(1,128)S(1)} %get-tuple-element.25.after_ref.taps_ref, ...), custom_call_target="tpu_custom_call" | custom-call | flops 268435456 | tf_op jit(solution)/shard_map/mix/pallas_call | solution.py:33
  28.3 11.1 %all_to_all.26.mixed_ref = bf16[16,8,1024]{2,1,0:T(8,128)(2,1)S(1)} all-to-all(bf16[16,8,1024]{2,1,0:T(8,128)(2,1)S(1)} %get-tuple-element.33), channel_id=1, replica_groups=mesh['dp'=4,'kv'=16,'tp'=2] {'kv'}, dimensions={0} | all-to-all | bytes 524288 | tf_op jit(solution)/shard_map/all_to_all | solution.py:27
  39.4 0.5 mix_out.1
  39.9 12.2 %all_to_all.27.cols_ref = bf16[16,64,256]{2,1,0:T(8,128)(2,1)S(1)} all-to-all(bf16[16,64,256]{2,1,0:T(8,128)(2,1)S(1)} %mix_out.1), channel_id=1, replica_groups=mesh['dp'=4,'kv'=16,'tp'=2] {'kv'}, dimensions={0} | all-to-all | bytes 1048576 | tf_op jit(solution)/shard_map/all_to_all | solution.py:27
  52.1 0.0 copy-start.5
  52.1 4.2 %channel_mixer.1 = (bf16[16,8,2048]{2,1,0:T(8,128)(2,1)S(1)}, f32[8,2048]{1,0:T(8,128)S(1)}, f32[8192,128]{1,0:T(8,128)}) custom-call(bf16[16,64,256]{2,1,0:T(8,128)(2,1)S(1)} %all_to_all.27.cols_ref, f32[1,4096]{1,0:T(1,128)S(1)} %bitcast.15, bf16[4096,512]{1,0:T(8,128)(2,1)S(1)} %copy-done.1, bf16[4096,512]{1,0:T(8,128)(2,1)S(1)} %collective-permute-done.2.up_far_ref, ...), custom_call_target="tpu_custom_call" | custom-call | flops 2147483648 | tf_op jit(solution)/shard_map/channel_mixer/pallas_call | solution.py:33
  56.3 11.8 %all_to_all.28.arrived_ref = bf16[16,8,2048]{2,1,0:T(8,128)(2,1)S(1)} all-to-all(bf16[16,8,2048]{2,1,0:T(8,128)(2,1)S(1)} %get-tuple-element.41), channel_id=1, replica_groups=mesh['dp'=4,'kv'=16,'tp'=2] {'kv'}, dimensions={0} | all-to-all | bytes 1048576 | tf_op jit(solution)/shard_map/all_to_all | solution.py:27
  68.1 0.4 last_norm.1
  68.5 14.9 %all_to_all.29 = bf16[32,4,128]{2,1,0:T(4,128)(2,1)S(1)} all-to-all(bf16[32,4,128]{2,1,0:T(4,128)(2,1)S(1)} %last_norm.1), channel_id=1, replica_groups=mesh['dp'=4,'kv'=16,'tp'=2] {'kv','tp'}, dimensions={0} | all-to-all | bytes 65536 | tf_op jit(solution)/shard_map/all_to_all | solution.py:27
  83.4 0.6 copy.25
  (11 shorter events, 0.0 us)
Async XLA Ops:
  0.6 26.8 %copy-start.6 = (f32[2048]{0:T(1024)S(1)}, f32[2048]{0:T(1024)}, u32[]{:S(2)}) copy-start(f32[2048]{0:T(1024)} %param.38) | copy-start | bytes 24580
  0.6 26.8 %copy-start = (f32[4,32,64,128]{3,2,1,0:T(8,128)S(1)}, f32[4,32,64,128]{3,2,1,0:T(8,128)}, u32[]{:S(2)}) copy-start(f32[4,32,64,128]{3,2,1,0:T(8,128)} %param.37) | copy-start | bytes 12582916
  2.9 3.2 %collective-permute-start = (bf16[16,8,2560]{2,1,0:T(8,128)(2,1)S(1)}, bf16[16,8,2560]{2,1,0:T(8,128)(2,1)S(1)}, u32[]{:S(2)}, u32[]{:S(2)}) collective-permute-start(bf16[16,8,2560]{2,1,0:T(8,128)(2,1)S(1)} %get-tuple-element.24), channel_id=1, source_target_pairs={{0,1},{1,0},{2,3},{3,2},{4,5},{5,4},{6,7},{7,6},{8,9},{9,8},{10,11... | collective-permute-start | bytes 1966088 | tf_op jit(solution)/shard_map/ppermute | solution.py:23
  4.3 2.5 %collective-permute-start.1 = (bf16[2048,128]{1,0:T(8,128)(2,1)}, bf16[2048,128]{1,0:T(8,128)(2,1)S(1)}, u32[]{:S(2)}, u32[]{:S(2)}) collective-permute-start(bf16[2048,128]{1,0:T(8,128)(2,1)} %own_weight_ref.1), channel_id=1, source_target_pairs={{0,1},{1,0},{2,3},{3,2},{4,5},{5,4},{6,7},{7,6},{8,9},{9,8},{10,11... | collective-permute-start | bytes 1572872 | tf_op jit(solution)/shard_map/ppermute | solution.py:23
  6.0 33.3 %copy-start.3 = (bf16[2048,128]{1,0:T(8,128)(2,1)S(1)}, bf16[2048,128]{1,0:T(8,128)(2,1)}, u32[]{:S(2)}) copy-start(bf16[2048,128]{1,0:T(8,128)(2,1)} %own_weight_ref.1) | copy-start | bytes 1572868
  6.8 20.6 %collective-permute-start.2 = (bf16[4096,512]{1,0:T(8,128)(2,1)}, bf16[4096,512]{1,0:T(8,128)(2,1)S(1)}, u32[]{:S(2)}, u32[]{:S(2)}) collective-permute-start(bf16[4096,512]{1,0:T(8,128)(2,1)} %up_own_ref.1), channel_id=1, source_target_pairs={{0,1},{1,0},{2,3},{3,2},{4,5},{5,4},{6,7},{7,6},{8,9},{9,8},{10,11... | collective-permute-start | bytes 12582920 | tf_op jit(solution)/shard_map/ppermute | solution.py:23
  7.2 20.2 %collective-permute-start.3 = (bf16[512,4096]{1,0:T(8,128)(2,1)}, bf16[512,4096]{1,0:T(8,128)(2,1)S(1)}, u32[]{:S(2)}, u32[]{:S(2)}) collective-permute-start(bf16[512,4096]{1,0:T(8,128)(2,1)} %down_own_ref.1), channel_id=1, source_target_pairs={{0,1},{1,0},{2,3},{3,2},{4,5},{5,4},{6,7},{7,6},{8,9},{9,8},{10,11... | collective-permute-start | bytes 12582920 | tf_op jit(solution)/shard_map/ppermute | solution.py:23
  27.4 24.6 %copy-start.1 = (bf16[4096,512]{1,0:T(8,128)(2,1)S(1)}, bf16[4096,512]{1,0:T(8,128)(2,1)}, u32[]{:S(2)}) copy-start(bf16[4096,512]{1,0:T(8,128)(2,1)} %up_own_ref.1) | copy-start | bytes 12582916
  27.4 24.6 %copy-start.2 = (bf16[512,4096]{1,0:T(8,128)(2,1)S(1)}, bf16[512,4096]{1,0:T(8,128)(2,1)}, u32[]{:S(2)}) copy-start(bf16[512,4096]{1,0:T(8,128)(2,1)} %down_own_ref.1) | copy-start | bytes 12582916
  27.4 24.6 %copy-start.4 = (f32[4096]{0:T(1024)S(1)}, f32[4096]{0:T(1024)}, u32[]{:S(2)}) copy-start(f32[4096]{0:T(1024)} %param.40) | copy-start | bytes 49156
  52.1 16.1 %copy-start.5 = (f32[4096]{0:T(1024)S(1)}, f32[4096]{0:T(1024)}, u32[]{:S(2)}) copy-start(f32[4096]{0:T(1024)} %param.43) | copy-start | bytes 49156
